TPU v7x, 128 devices: a whole 4x4x4 slice. The times are simulated.
128 devices in a mesh: ep: 64 (over z, y, x), tp: 2 (over core).
Axes of the slice: x: 4, y: 4, z: 4, core: 2. Of those that a mesh axis runs over, the one named last changes fastest.
Arguments:
- hidden_in: bfloat16 [2048, 2048], P('ep'), may hold values from -6 to 6
- past_lengths: int32 [2048], P('ep'), may hold values from 1 to 1023, as said below
- key_cache: bfloat16 [2048, 1024, 256], P('ep', None, 'tp'), may hold values from -512 to 512
- value_cache: bfloat16 [2048, 1024, 256], P('ep', None, 'tp'), may hold values from -6 to 6
- attn_gain: float32 [2048], replicated, may hold values from 0.1 to 1.9
- w_query: bfloat16 [2048, 2048], P(None, 'tp'), may hold values from -0.125 to 0.125
- w_key: bfloat16 [2048, 256], P(None, 'tp'), may hold values from -0.125 to 0.125
- w_value: bfloat16 [2048, 256], P(None, 'tp'), may hold values from -0.125 to 0.125
- lambdas: float32 [16], P('tp'), may hold values from 0.3 to 0.8
- head_gain: float32 [128], replicated, may hold values from 0.1 to 1.9
- w_out: bfloat16 [2048, 2048], P('tp'), may hold values from -0.125 to 0.125
- ffn_gain: float32 [2048], replicated, may hold values from 0.1 to 1.9
- route_ids: int32 [2048, 2], P('ep'), may hold values from 0 to 31, all different within a row; in each aligned block of 32 rows (0 to 31, 32 to 63, ...) at most 4 rows name the same one
- route_weights: float32 [2048, 2], P('ep'), may hold values from 0.2 to 1
- expert_gate: bfloat16 [64, 2048, 704], P('ep', None, 'tp'), may hold values from -0.125 to 0.125
- expert_up: bfloat16 [64, 2048, 704], P('ep', None, 'tp'), may hold values from -0.125 to 0.125
- expert_down: bfloat16 [64, 704, 2048], P('ep', None, 'tp'), may hold values from -1.25 to 1.25
- gate_vector: bfloat16 [2048], replicated, may hold values from -0.125 to 0.125
- dense_gate: bfloat16 [2048, 5632], P(None, ('ep', 'tp')), may hold values from -0.125 to 0.125
- dense_up: bfloat16 [2048, 5632], P(None, ('ep', 'tp')), may hold values from -0.125 to 0.125
- dense_down: bfloat16 [5632, 2048], P('ep', 'tp'), may hold values from -0.625 to 0.625
Outputs:
- mixed_out: bfloat16 [2048, 2048], P('ep', 'tp')
- new_keys: bfloat16 [2048, 256], P('ep', 'tp')
- new_values: bfloat16 [2048, 256], P('ep', 'tp')
Inputs may be any that keep to these rules, and one draw needn't show every extreme that they name: `past_lengths`: the new token of a sequence stands at this position; some sequence has 1023 cached positions in every draw. `route_ids`: each row names 2 different experts; among the rows of one index of ep no expert is named more than 4 times, a bound that some block reaches in every draw.
All inputs are finite; a program needn't handle non-finite values.
Results may differ from a plain program's by a relative error of at most 0.02.
The roundings to bfloat16 on the way count: a program that leaves them out, or rounds other values in their place, can miss the bound.
Values may be sent and summed in bfloat16 or wider, within the bound.
No kernel may reach another device: no remote copies, remote signals or barrier semaphores. Data moves between devices by JAX's collectives and lax.ppermute only.
A program may use at most 128 MiB of HBM per device.

v0:
```python
import jax
import jax.numpy as jnp
from jax import lax
from jax.sharding import PartitionSpec as P

HEAD_DIM = 64
VALUE_DIM = 128


norm_eps = 1e-05
rope_base = 10000.0


def sent_to_all(x, axis):
    size = lax.axis_size(axis)
    return lax.all_to_all(jnp.broadcast_to(x[None], (size, *x.shape)), axis, 0, 0, tiled=True)


def taken_together(x, axis):
    return sent_to_all(x, axis).astype(jnp.float32).sum(axis=0)


def in_order(pieces, dim):
    pieces = jnp.moveaxis(pieces, 0, dim)
    shape = pieces.shape
    return pieces.reshape(*shape[:dim], shape[dim] * shape[dim + 1], *shape[dim + 2 :])


def collect(x, axis, dim):
    pieces = sent_to_all(x, axis)
    return in_order(pieces, dim)


def in_one_piece(arrays, axis, dim, along):
    columns = [a.reshape(*a.shape[:along], -1) for a in arrays]
    both = jnp.concatenate(columns, axis=along)
    filled, at, outs = (lax.all_gather(both, axis, axis=dim, tiled=True), 0, [])
    for a, column in zip(arrays, columns):
        piece = filled[..., at : at + column.shape[along]]
        outs.append(piece.reshape(*piece.shape[:along], *a.shape[along:]))
        at += column.shape[along]
    return tuple(outs)


def side_by_side(arrays, axis, split_dim, concat_dim, along):
    both = jnp.concatenate(arrays, axis=along)
    filled, at, outs = (
        lax.all_to_all(both, axis, split_axis=split_dim, concat_axis=concat_dim, tiled=True),
        0,
        [],
    )
    for a in arrays:
        outs.append(lax.slice_in_dim(filled, at, at + a.shape[along], axis=along))
        at += a.shape[along]
    return tuple(outs)


def cut_along(x, dim, size):
    shape = x.shape
    pieces = x.reshape(*shape[:dim], size, shape[dim] // size, *shape[dim + 1 :])
    return jnp.moveaxis(pieces, dim, 0)


def sum_at_owner(x, axis, dim):
    pieces = cut_along(x, dim, lax.axis_size(axis))
    arrived = lax.all_to_all(pieces, axis, split_axis=0, concat_axis=0, tiled=True)
    return arrived.astype(jnp.float32).sum(axis=0)


def rms_rows(values, scales):
    values = values.astype(jnp.float32)
    return values * lax.rsqrt(jnp.mean(values * values, axis=-1, keepdims=True) + norm_eps) * scales


def rotary(values, position):
    middle = values.shape[-1] // 2
    inverse = rope_base ** (-jnp.arange(middle, dtype=jnp.float32) / middle)
    angles = position.astype(jnp.float32)[:, None] * inverse[None, :]
    cosine = jnp.cos(angles)[:, None, None, :]
    sine_part = jnp.sin(angles)[:, None, None, :]
    leading, second = (values[..., :middle], values[..., middle:])
    return jnp.concatenate(
        [leading * cosine - second * sine_part, second * cosine + leading * sine_part], axis=-1
    )


def per_device(
    hidden_in,
    past_lengths,
    key_cache,
    value_cache,
    attn_gain,
    w_query,
    w_key,
    w_value,
    lambdas,
    head_gain,
    w_out,
    ffn_gain,
    route_ids,
    route_weights,
    expert_gate,
    expert_up,
    expert_down,
    gate_vector,
    dense_gate,
    dense_up,
    dense_down,
):
    batch_rows = hidden_in.shape[0]
    model_width = hidden_in.shape[1]
    tp_count = lax.axis_size("tp")
    ep_count = lax.axis_size("ep")
    tp_rank = lax.axis_index("tp")
    half_width = model_width // tp_count
    heads_here = lambdas.shape[0]
    kv_here = w_key.shape[1] // (2 * HEAD_DIM)
    per_key = heads_here // kv_here
    scale_qk = HEAD_DIM ** (-0.5)
    normed = rms_rows(hidden_in, attn_gain).astype(jnp.bfloat16)
    queries = rotary(
        jnp.dot(normed, w_query, preferred_element_type=jnp.float32).reshape(
            batch_rows, heads_here, 2, HEAD_DIM
        ),
        past_lengths,
    ).astype(jnp.bfloat16)
    key_new = rotary(
        jnp.dot(normed, w_key, preferred_element_type=jnp.float32).reshape(
            batch_rows, kv_here, 2, HEAD_DIM
        ),
        past_lengths,
    ).astype(jnp.bfloat16)
    value_new = jnp.dot(normed, w_value, preferred_element_type=jnp.float32).astype(jnp.bfloat16)
    grouped = queries.reshape(batch_rows, kv_here, per_key, 2, HEAD_DIM)
    own_score = (
        jnp.einsum("sgamd,sgmd->sgam", grouped, key_new, preferred_element_type=jnp.float32)
        * scale_qk
    )
    value_rows = value_new.reshape(batch_rows, kv_here, 1, 1, VALUE_DIM).astype(jnp.float32)
    start_state = (
        own_score,
        jnp.ones_like(own_score),
        jnp.broadcast_to(value_rows, own_score.shape + (VALUE_DIM,)),
    )
    cache_len = key_cache.shape[1]
    span_len = min(256, cache_len)
    spans_needed = (jnp.max(past_lengths) + span_len - 1) // span_len

    def visit(block_index, carried):
        running, totals, summed = carried
        offset = block_index * span_len
        key_rows = lax.dynamic_slice_in_dim(key_cache, offset, span_len, 1).reshape(
            batch_rows, span_len, kv_here, 2, HEAD_DIM
        )
        cached = lax.dynamic_slice_in_dim(value_cache, offset, span_len, 1).reshape(
            batch_rows, span_len, kv_here, VALUE_DIM
        )
        scores = (
            jnp.einsum("sgamd,slgmd->sgaml", grouped, key_rows, preferred_element_type=jnp.float32)
            * scale_qk
        )
        usable = (offset + jnp.arange(span_len))[None, :] < past_lengths[:, None]
        scores = jnp.where(usable[:, None, None, None, :], scores, -jnp.inf)
        raised = jnp.maximum(running, jnp.max(scores, axis=-1))
        fading = jnp.exp(running - raised)
        weights = jnp.exp(scores - raised[..., None])
        totals = totals * fading + jnp.sum(weights, axis=-1)
        summed = summed * fading[..., None] + jnp.einsum(
            "sgaml,slge->sgame",
            weights.astype(jnp.bfloat16),
            cached,
            preferred_element_type=jnp.float32,
        )
        return (raised, totals, summed)

    running, totals, summed = lax.fori_loop(0, spans_needed, visit, start_state)
    mapped = summed / totals[..., None]
    head_mix = mapped[..., 0, :] - lambdas.reshape(1, kv_here, per_key, 1) * mapped[..., 1, :]
    head_out = rms_rows(head_mix, head_gain).astype(jnp.bfloat16).reshape(batch_rows, -1)
    attn_out = (
        taken_together(
            jnp.dot(head_out, w_out, preferred_element_type=jnp.float32).astype(jnp.bfloat16), "tp"
        )
        .astype(jnp.float32)
        .astype(jnp.bfloat16)
    )
    residual = hidden_in.astype(jnp.float32) + attn_out.astype(jnp.float32)
    moe_in = rms_rows(residual, ffn_gain).astype(jnp.bfloat16)
    mix_gate = jax.nn.sigmoid(
        jnp.dot(moe_in, gate_vector, preferred_element_type=jnp.float32)
    ).astype(jnp.bfloat16)
    top_count = route_ids.shape[1]
    experts = ep_count // 2
    capacity = max(2, 2 * batch_rows * top_count // experts)
    flat_ids = route_ids.reshape(-1)
    matches = (flat_ids[:, None] == jnp.arange(experts)[None, :]).astype(jnp.int32)
    earlier = jnp.sum((jnp.cumsum(matches, axis=0) - matches) * matches, axis=1)
    slot_of = flat_ids * capacity + earlier
    placing = (jnp.arange(experts * capacity)[:, None] == slot_of[None, :]).astype(jnp.float32)
    repeated = jnp.repeat(moe_in, top_count, axis=0)
    packed = jnp.dot(
        placing.astype(jnp.bfloat16), repeated, preferred_element_type=jnp.float32
    ).astype(jnp.bfloat16)
    outgoing = jnp.broadcast_to(
        packed.reshape(experts, 1, capacity, model_width), (experts, 2, capacity, model_width)
    ).reshape(ep_count, capacity, model_width)
    arrived = lax.all_to_all(outgoing, "ep", split_axis=0, concat_axis=0, tiled=True)
    leading = arrived.shape[:2]
    flat_rows = arrived.reshape(-1, model_width)
    gate_pre = jnp.dot(flat_rows, expert_gate[0], preferred_element_type=jnp.float32)
    up_pre = jnp.dot(flat_rows, expert_up[0], preferred_element_type=jnp.float32)
    inner_act = (jax.nn.silu(gate_pre) * up_pre).astype(jnp.bfloat16)
    inner_act = collect(inner_act, "tp", 1)
    partial_value = jnp.dot(inner_act, expert_down[0], preferred_element_type=jnp.float32).reshape(
        leading + (half_width,)
    )
    returned = lax.all_to_all(
        partial_value.astype(jnp.bfloat16), "ep", split_axis=0, concat_axis=0, tiled=True
    ).astype(partial_value.dtype)
    paired = jnp.sum(returned.reshape(experts, 2, capacity, half_width), axis=1).reshape(
        experts * capacity, half_width
    )
    weighted = (
        (placing * route_weights.reshape(1, -1))
        .reshape(experts * capacity, batch_rows, top_count)
        .sum(axis=2)
    )
    moe_out = jnp.einsum("ct,cd->td", weighted, paired, precision=lax.Precision.HIGHEST)
    own_half = lax.dynamic_slice_in_dim(moe_in, tp_rank * half_width, half_width, 1)
    rows_all, gates_all = in_one_piece((own_half, mix_gate), "ep", 0, 1)
    columns = dense_gate.shape[1]
    gate_cols, up_cols = side_by_side(
        (
            dense_gate.reshape(tp_count, half_width, columns),
            dense_up.reshape(tp_count, half_width, columns),
        ),
        "tp",
        0,
        2,
        1,
    )
    pre_gate, pre_up = (
        taken_together(
            jnp.dot(rows_all, gate_cols[0], preferred_element_type=jnp.float32).astype(
                jnp.bfloat16
            ),
            "tp",
        ).astype(jnp.float32),
        taken_together(
            jnp.dot(rows_all, up_cols[0], preferred_element_type=jnp.float32).astype(jnp.bfloat16),
            "tp",
        ).astype(jnp.float32),
    )
    dense_act = (jax.nn.silu(pre_gate) * pre_up).astype(jnp.bfloat16)
    gate_rows = gates_all.astype(jnp.float32)
    dense_out = sum_at_owner(
        (
            jnp.dot(dense_act, dense_down, preferred_element_type=jnp.float32) * gate_rows[:, None]
        ).astype(jnp.bfloat16),
        "ep",
        0,
    )
    own_residual = lax.dynamic_slice_in_dim(residual, tp_rank * half_width, half_width, 1)
    mixed_out = (own_residual + moe_out + dense_out).astype(jnp.bfloat16)
    return (mixed_out, key_new.reshape(batch_rows, -1), value_new)


def solution(mesh):
    return jax.shard_map(
        per_device,
        mesh=mesh,
        in_specs=(
            P("ep", None),
            P("ep"),
            P("ep", None, "tp"),
            P("ep", None, "tp"),
            P(),
            P(None, "tp"),
            P(None, "tp"),
            P(None, "tp"),
            P("tp"),
            P(),
            P("tp", None),
            P(),
            P("ep", None),
            P("ep", None),
            P("ep", None, "tp"),
            P("ep", None, "tp"),
            P("ep", None, "tp"),
            P(),
            P(None, ("ep", "tp")),
            P(None, ("ep", "tp")),
            P("ep", "tp"),
        ),
        out_specs=(P("ep", "tp"), P("ep", "tp"), P("ep", "tp")),
        check_vma=False,
    )
```

profile of v0, /device:TPU:0, one launch (start us, length us, event | category | flops | bytes accessed | tf_op | source)
XLA Modules:
  0.0 275.9 jit_solution(12817063429684109780)
XLA Ops:
  7.2 1.5 fusion.80
  10.4 3.2 %fusion.73 = f32[32,1024]{1,0:T(8,128)S(1)} fusion(bf16[2048,1024]{1,0:T(8,128)(2,1)} %param.28, bf16[32,2048]{1,0:T(8,128)(2,1)} %param.23, f32[2048]{0:T(1024)} %param.27, f32[32]{0:T(128)S(1)} %add_rsqrt_fusion.2), kind=kOutput, calls=%fused_computation.116 | convolution fusion | flops 134479872 | bytes 4464768 | tf_op jit(solution)/shard_map/dot_general | solution.py:122
  18.3 57.8 %while.14 = (s32[]{:T(128)}, f32[32,1,8,2]{2,3,0,1:T(2,128)}, f32[32,1,8,2]{2,3,0,1:T(2,128)}, f32[32,1,8,2,128]{4,2,3,0,1:T(8,128)}, s32[]{:T(128)}, /*index=5*...) while((s32[]{:T(128)}, f32[32,1,8,2]{2,3,0,1:T(2,128)}, ...), condition=%wide.region_5.6_spmd, body=%wide.region_2.5_spmd.sunk | while | flops 51390212 | bytes 14797119 | solution.py:176
  18.3 3.1 %constant_dynamic-slice_fusion.3 = bf16[32,256,128]{2,1,0:T(8,128)(2,1)} fusion(bf16[32,1024,128]{2,1,0:T(8,128)(2,1)} %get-tuple-element.251, s32[]{:T(128)S(6)} %select_n.26), kind=kLoop, calls=%fused_computation.22.clone.1 | loop fusion | bytes 4194308 | tf_op jit(solution)/shard_map/while/body/dynamic_slice | solution.py:152
  21.4 3.3 %copy.152 = bf16[32,256,128]{1,2,0:T(8,128)(2,1)S(1)} copy(bf16[32,256,128]{2,1,0:T(8,128)(2,1)} %constant_dynamic-slice_fusion.3) | data formatting | bytes 4194304 | tf_op jit(solution)/shard_map/while/body/dynamic_slice | solution.py:152
  25.4 1.4 fusion.104
  27.9 1.4 bitcast_add_fusion.2
  30.0 2.8 %fusion.107 = f32[32,1,8,2,128]{4,2,3,0,1:T(8,128)} fusion(bf16[32,1024,128]{2,1,0:T(8,128)(2,1)} %get-tuple-element.253, s32[]{:T(128)S(6)} %select_n.26, f32[32,1,8,2,256]{4,2,3,0,1:T(8,128)S(1)} %get-tuple-element.217, f32[32,1,8,2,128]{4,2,3,0,1:T(8,128)} %get-tuple-element.235, f32[32,8,2]{1,2,0:T(2,128)S(1)} %bitcast.179, ...), kind=kOutput, calls=%fused_computation.8.clone.1 | convolution fusion | flops 33947648 | bytes 3149828 | tf_op jit(solution)/shard_map/while/body/sgaml,slge->sgame/dot_general | solution.py:168
  32.7 3.1 %constant_dynamic-slice_fusion.3 = bf16[32,256,128]{2,1,0:T(8,128)(2,1)} fusion(bf16[32,1024,128]{2,1,0:T(8,128)(2,1)} %get-tuple-element.251, s32[]{:T(128)S(6)} %select_n.26), kind=kLoop, calls=%fused_computation.22.clone.1 | loop fusion | bytes 4194308 | tf_op jit(solution)/shard_map/while/body/dynamic_slice | solution.py:152
  35.9 3.3 %copy.152 = bf16[32,256,128]{1,2,0:T(8,128)(2,1)S(1)} copy(bf16[32,256,128]{2,1,0:T(8,128)(2,1)} %constant_dynamic-slice_fusion.3) | data formatting | bytes 4194304 | tf_op jit(solution)/shard_map/while/body/dynamic_slice | solution.py:152
  39.9 1.4 fusion.104
  42.4 1.4 bitcast_add_fusion.2
  44.4 2.8 %fusion.107 = f32[32,1,8,2,128]{4,2,3,0,1:T(8,128)} fusion(bf16[32,1024,128]{2,1,0:T(8,128)(2,1)} %get-tuple-element.253, s32[]{:T(128)S(6)} %select_n.26, f32[32,1,8,2,256]{4,2,3,0,1:T(8,128)S(1)} %get-tuple-element.217, f32[32,1,8,2,128]{4,2,3,0,1:T(8,128)} %get-tuple-element.235, f32[32,8,2]{1,2,0:T(2,128)S(1)} %bitcast.179, ...), kind=kOutput, calls=%fused_computation.8.clone.1 | convolution fusion | flops 33947648 | bytes 3149828 | tf_op jit(solution)/shard_map/while/body/sgaml,slge->sgame/dot_general | solution.py:168
  47.2 3.1 %constant_dynamic-slice_fusion.3 = bf16[32,256,128]{2,1,0:T(8,128)(2,1)} fusion(bf16[32,1024,128]{2,1,0:T(8,128)(2,1)} %get-tuple-element.251, s32[]{:T(128)S(6)} %select_n.26), kind=kLoop, calls=%fused_computation.22.clone.1 | loop fusion | bytes 4194308 | tf_op jit(solution)/shard_map/while/body/dynamic_slice | solution.py:152
  50.3 3.3 %copy.152 = bf16[32,256,128]{1,2,0:T(8,128)(2,1)S(1)} copy(bf16[32,256,128]{2,1,0:T(8,128)(2,1)} %constant_dynamic-slice_fusion.3) | data formatting | bytes 4194304 | tf_op jit(solution)/shard_map/while/body/dynamic_slice | solution.py:152
  54.4 1.4 fusion.104
  56.8 1.4 bitcast_add_fusion.2
  58.9 2.8 %fusion.107 = f32[32,1,8,2,128]{4,2,3,0,1:T(8,128)} fusion(bf16[32,1024,128]{2,1,0:T(8,128)(2,1)} %get-tuple-element.253, s32[]{:T(128)S(6)} %select_n.26, f32[32,1,8,2,256]{4,2,3,0,1:T(8,128)S(1)} %get-tuple-element.217, f32[32,1,8,2,128]{4,2,3,0,1:T(8,128)} %get-tuple-element.235, f32[32,8,2]{1,2,0:T(2,128)S(1)} %bitcast.179, ...), kind=kOutput, calls=%fused_computation.8.clone.1 | convolution fusion | flops 33947648 | bytes 3149828 | tf_op jit(solution)/shard_map/while/body/sgaml,slge->sgame/dot_general | solution.py:168
  61.7 3.1 %constant_dynamic-slice_fusion.3 = bf16[32,256,128]{2,1,0:T(8,128)(2,1)} fusion(bf16[32,1024,128]{2,1,0:T(8,128)(2,1)} %get-tuple-element.251, s32[]{:T(128)S(6)} %select_n.26), kind=kLoop, calls=%fused_computation.22.clone.1 | loop fusion | bytes 4194308 | tf_op jit(solution)/shard_map/while/body/dynamic_slice | solution.py:152
  64.8 3.3 %copy.152 = bf16[32,256,128]{1,2,0:T(8,128)(2,1)S(1)} copy(bf16[32,256,128]{2,1,0:T(8,128)(2,1)} %constant_dynamic-slice_fusion.3) | data formatting | bytes 4194304 | tf_op jit(solution)/shard_map/while/body/dynamic_slice | solution.py:152
  68.8 1.4 fusion.104
  71.3 1.4 bitcast_add_fusion.2
  73.3 2.8 %fusion.107 = f32[32,1,8,2,128]{4,2,3,0,1:T(8,128)} fusion(bf16[32,1024,128]{2,1,0:T(8,128)(2,1)} %get-tuple-element.253, s32[]{:T(128)S(6)} %select_n.26, f32[32,1,8,2,256]{4,2,3,0,1:T(8,128)S(1)} %get-tuple-element.217, f32[32,1,8,2,128]{4,2,3,0,1:T(8,128)} %get-tuple-element.235, f32[32,8,2]{1,2,0:T(2,128)S(1)} %bitcast.179, ...), kind=kOutput, calls=%fused_computation.8.clone.1 | convolution fusion | flops 33947648 | bytes 3149828 | tf_op jit(solution)/shard_map/while/body/sgaml,slge->sgame/dot_general | solution.py:168
  76.1 1.1 broadcast_divide_fusion
  79.1 3.0 %convolution_convert_fusion.1 = bf16[32,2048]{1,0:T(8,128)(2,1)S(1)} fusion(bf16[1024,2048]{1,0:T(8,128)(2,1)} %param.33, f32[4,8,8,128]{3,2,1,0:T(8,128)S(1)} %bitcast.186, f32[4,8,8,128]{3,2,1,0:T(8,128)S(1)} %bitcast.188, f32[4,8,8,128]{3,2,1,0:T(8,128)S(1)} %bitcast.187, f32[1024]{0:T(1024)S(1)} %get-tuple-element.153, f32[1024]{0:T(1024)S(1)} %get-tuple-element.154), kind=kOutput, calls=%fused_computation.32 | convolution fusion | flops 134447104 | bytes 4726784 | tf_op jit(solution)/shard_map/dot_general | solution.py:182
  82.8 3.4 %all-to-all-start = ((bf16[2,32,2048]{2,1,0:T(8,128)(2,1)}), bf16[2,32,2048]{2,1,0:T(8,128)(2,1)S(1)}, u32[]{:S(2)}, u32[]{:S(2)}) async-start(bf16[2,32,2048]{2,1,0:T(8,128)(2,1)} %broadcast_in_dim.37), calls=%async_computation | async-start | bytes 524288 | tf_op jit(solution)/shard_map/all_to_all | solution.py:16
  86.3 1.5 all-to-all-done
  90.9 3.5 %all-to-all-start.4 = ((bf16[2,2048,44]{1,2,0:T(8,128)(2,1)}), bf16[2,2048,44]{1,2,0:T(8,128)(2,1)S(1)}, u32[]{:S(2)}, u32[]{:S(2)}) async-start(bf16[2,2048,44]{1,2,0:T(8,128)(2,1)} %pad_maximum_fusion), calls=%async_computation.4 | async-start | bytes 786432 | tf_op jit(solution)/shard_map/all_to_all | solution.py:48
  96.2 1.6 broadcast_in_dim.40
  97.8 11.5 %all-to-all-start.1 = ((bf16[64,4,2048]{2,1,0:T(4,128)(2,1)}), bf16[64,4,2048]{2,1,0:T(4,128)(2,1)S(1)}, u32[]{:S(2)}, u32[]{:S(2)}) async-start(bf16[64,4,2048]{2,1,0:T(4,128)(2,1)} %bitcast.26), calls=%async_computation.1 | async-start | bytes 2097152 | tf_op jit(solution)/shard_map/all_to_all | solution.py:207
  110.2 18.8 %all-to-all-done.1 = bf16[64,4,2048]{2,1,0:T(4,128)(2,1)S(1)} async-done(((bf16[64,4,2048]{2,1,0:T(4,128)(2,1)}), bf16[64,4,2048]{2,1,0:T(4,128)(2,1)S(1)}, u32[]{:S(2)}, u32[]{:S(2)}) %all-to-all-start.1) | async-done | bytes 1048608 | tf_op jit(solution)/shard_map/all_to_all | solution.py:207
  129.3 1.9 fusion.34
  131.2 1.9 fusion.42
  133.2 4.1 %all_to_all.53 = bf16[2,256,352]{1,2,0:T(8,128)(2,1)S(1)} all-to-all(bf16[2,256,352]{1,2,0:T(8,128)(2,1)S(1)} %broadcast_in_dim.41), channel_id=1, replica_groups=mesh['ep'=64,'tp'=2] {'tp'}, dimensions={0} | all-to-all | bytes 720896 | tf_op jit(solution)/shard_map/all_to_all | solution.py:16
  138.8 1.2 copy.120
  140.0 28.0 %all-gather.2.cloned.1.call-done = bf16[2048,1025]{1,0:T(8,128)(2,1)} async-done(((bf16[32,1025]{1,0:T(8,128)(2,1)}), bf16[2048,1025]{1,0:T(8,128)(2,1)}) %all-gather.2.cloned.1.call-update) | async-done | bytes 4198416 | tf_op jit(solution)/shard_map/all_gather | solution.py:37
  168.0 3.6 %fusion.27 = bf16[2048,88]{0,1:T(8,128)(2,1)S(1)} fusion(bf16[2048,1025]{1,0:T(8,128)(2,1)} %all-gather.2.cloned.1.call-done, bf16[1,2048,88]{1,2,0:T(8,128)(2,1)S(1)} %copy-done.6), kind=kOutput, calls=%fused_computation.31 | convolution fusion | flops 369278976 | bytes 4734976 | tf_op jit(solution)/shard_map/dot_general | solution.py:250
  172.6 3.7 %all-to-all-start.6 = ((bf16[2,2048,88]{1,2,0:T(8,128)(2,1)}), bf16[2,2048,88]{1,2,0:T(8,128)(2,1)S(1)}, u32[]{:S(2)}, u32[]{:S(2)}) async-start(bf16[2,2048,88]{1,2,0:T(8,128)(2,1)} %broadcast_in_dim.43), calls=%async_computation.6 | async-start | bytes 1441792 | tf_op jit(solution)/shard_map/all_to_all | solution.py:16
  176.3 3.6 %fusion.24 = bf16[2048,88]{0,1:T(8,128)(2,1)S(1)} fusion(bf16[2048,1025]{1,0:T(8,128)(2,1)} %all-gather.2.cloned.1.call-done, bf16[1,2048,88]{1,2,0:T(8,128)(2,1)S(1)} %copy-done.6), kind=kOutput, calls=%fused_computation.30 | convolution fusion | flops 369278976 | bytes 4734976 | tf_op jit(solution)/shard_map/dot_general | solution.py:244
  180.9 3.5 %all-to-all-start.5 = ((bf16[2,2048,88]{1,2,0:T(8,128)(2,1)}), bf16[2,2048,88]{1,2,0:T(8,128)(2,1)S(1)}, u32[]{:S(2)}, u32[]{:S(2)}) async-start(bf16[2,2048,88]{1,2,0:T(8,128)(2,1)} %broadcast_in_dim.42), calls=%async_computation.5 | async-start | bytes 1441792 | tf_op jit(solution)/shard_map/all_to_all | solution.py:16
  186.3 6.5 %all-to-all-start.3 = ((bf16[64,4,1024]{2,1,0:T(4,128)(2,1)}), bf16[64,4,1024]{2,1,0:T(4,128)(2,1)S(1)}, u32[]{:S(2)}, u32[]{:S(2)}) async-start(bf16[64,4,1024]{2,1,0:T(4,128)(2,1)} %copy.120), calls=%async_computation.3 | async-start | bytes 1048576 | tf_op jit(solution)/shard_map/all_to_all | solution.py:217
  192.9 1.3 convert_reduce_fusion.4
  194.2 4.4 %multiply_convert_fusion = bf16[2048,1024]{1,0:T(8,128)(2,1)} fusion(bf16[88,1024]{1,0:T(8,128)(2,1)S(1)} %copy-done.20, f32[2048]{0:T(1024)S(1)} %convert_reduce_fusion.4, f32[2048,88]{0,1:T(8,128)} %convert_reduce_fusion.1, f32[2048,88]{0,1:T(8,128)S(1)} %convert_reduce_fusion.2), kind=kOutput, calls=%fused_computation.24 | convolution fusion | flops 374374400 | bytes 5824512 | tf_op jit(solution)/shard_map/dot_general | solution.py:258
  198.6 7.9 %all-to-all-done.3 = bf16[64,4,1024]{2,1,0:T(4,128)(2,1)S(1)} async-done(((bf16[64,4,1024]{2,1,0:T(4,128)(2,1)}), bf16[64,4,1024]{2,1,0:T(4,128)(2,1)S(1)}, u32[]{:S(2)}, u32[]{:S(2)}) %all-to-all-start.3) | async-done | bytes 524320 | tf_op jit(solution)/shard_map/all_to_all | solution.py:217
  206.4 5.8 %all-to-all-start.7 = ((bf16[64,32,1024]{2,1,0:T(8,128)(2,1)}), bf16[64,32,1024]{2,1,0:T(8,128)(2,1)}, u32[]{:S(2)}, u32[]{:S(2)}) async-start(bf16[64,32,1024]{2,1,0:T(8,128)(2,1)} %bitcast.180), calls=%async_computation.7 | async-start | bytes 8388608 | tf_op jit(solution)/shard_map/all_to_all | solution.py:66
  213.8 51.1 %all-to-all-done.7 = bf16[64,32,1024]{2,1,0:T(8,128)(2,1)} async-done(((bf16[64,32,1024]{2,1,0:T(8,128)(2,1)}), bf16[64,32,1024]{2,1,0:T(8,128)(2,1)}, u32[]{:S(2)}, u32[]{:S(2)}) %all-to-all-start.7) | async-done | bytes 4194336 | tf_op jit(solution)/shard_map/all_to_all | solution.py:66
  264.9 3.0 %convert_reduce_fusion = f32[32,1024]{1,0:T(8,128)S(1)} fusion(bf16[64,32,1024]{2,1,0:T(8,128)(2,1)} %all-to-all-done.7), kind=kLoop, calls=%fused_computation.23 | loop fusion | flops 4161536 | bytes 4325376 | tf_op jit(solution)/shard_map/reduce_sum | solution.py:67
  268.0 1.0 fusion.46
  (132 shorter events, 30.8 us)
Async XLA Ops:
  7.2 131.1 %copy-start = (bf16[1,704,1024]{2,1,0:T(8,128)(2,1)S(1)}, bf16[1,704,1024]{2,1,0:T(8,128)(2,1)}, u32[]{:S(2)}) copy-start(bf16[1,704,1024]{2,1,0:T(8,128)(2,1)} %param.39) | copy-start | bytes 4325380
  7.2 6.9 %copy-start.1 = (bf16[32,2048]{1,0:T(8,128)(2,1)S(1)}, bf16[32,2048]{1,0:T(8,128)(2,1)}, u32[]{:S(2)}) copy-start(bf16[32,2048]{1,0:T(8,128)(2,1)} %param.23) | copy-start | bytes 393220
  7.2 6.9 %copy-start.11 = (f32[2048]{0:T(1024)S(1)}, f32[2048]{0:T(1024)}, u32[]{:S(2)}) copy-start(f32[2048]{0:T(1024)} %param.27) | copy-start | bytes 24580
  7.2 6.9 %copy-start.4 = (bf16[2048,128]{1,0:T(8,128)(2,1)S(1)}, bf16[2048,128]{1,0:T(8,128)(2,1)}, u32[]{:S(2)}) copy-start(bf16[2048,128]{1,0:T(8,128)(2,1)} %param.29) | copy-start | bytes 1572868
  7.2 8.7 %copy-start.5 = (bf16[2048,128]{1,0:T(8,128)(2,1)S(1)}, bf16[2048,128]{1,0:T(8,128)(2,1)}, u32[]{:S(2)}) copy-start(bf16[2048,128]{1,0:T(8,128)(2,1)} %param.30) | copy-start | bytes 1572868
  14.8 3.5 %copy-start.9 = (bf16[32,1,2,32]{3,2,0,1:T(2,128)(2,1)}, bf16[32,1,2,32]{3,2,0,1:T(2,128)(2,1)S(1)}, u32[]{:S(2)}) copy-start(bf16[32,1,2,32]{3,2,0,1:T(2,128)(2,1)S(1)} %get-tuple-element.148) | copy-start | bytes 12292
  16.1 2.1 copy-start.12
  76.1 11.7 %copy-start.2 = (bf16[32,2048]{1,0:T(8,128)(2,1)S(1)}, bf16[32,2048]{1,0:T(8,128)(2,1)}, u32[]{:S(2)}) copy-start(bf16[32,2048]{1,0:T(8,128)(2,1)} %param.23) | copy-start | bytes 393220
  76.1 12.6 %copy-start.14 = (bf16[2048]{0:T(1024)(128)(2,1)S(1)}, bf16[2048]{0:T(1024)(128)(2,1)}, u32[]{:S(2)}) copy-start(bf16[2048]{0:T(1024)(128)(2,1)} %param.40) | copy-start | bytes 12292
  76.1 12.6 %copy-start.13 = (f32[2048]{0:T(1024)S(1)}, f32[2048]{0:T(1024)}, u32[]{:S(2)}) copy-start(f32[2048]{0:T(1024)} %param.34) | copy-start | bytes 24580
  77.3 12.5 %copy-start.7 = (bf16[2048,44]{0,1:T(8,128)(2,1)S(1)}, bf16[2048,44]{0,1:T(8,128)(2,1)}, u32[]{:S(2)}) copy-start(bf16[2048,44]{0,1:T(8,128)(2,1)} %param.42) | copy-start | bytes 540676
  79.0 11.0 %copy-start.8 = (bf16[2048,44]{0,1:T(8,128)(2,1)S(1)}, bf16[2048,44]{0,1:T(8,128)(2,1)}, u32[]{:S(2)}) copy-start(bf16[2048,44]{0,1:T(8,128)(2,1)} %param.41) | copy-start | bytes 540676
  79.1 15.3 %copy-start.15 = (s32[32,2]{0,1:T(2,128)S(1)}, s32[32,2]{0,1:T(2,128)}, u32[]{:S(2)}) copy-start(s32[32,2]{0,1:T(2,128)} %param.35) | copy-start | bytes 772
  82.8 5.0 %all-to-all-start = ((bf16[2,32,2048]{2,1,0:T(8,128)(2,1)}), bf16[2,32,2048]{2,1,0:T(8,128)(2,1)S(1)}, u32[]{:S(2)}, u32[]{:S(2)}) async-start(bf16[2,32,2048]{2,1,0:T(8,128)(2,1)} %broadcast_in_dim.37), calls=%async_computation | async-start | bytes 524288 | tf_op jit(solution)/shard_map/all_to_all | solution.py:16
  86.2 81.8 %all-gather.2.cloned.1.call-start = ((), (), s32[]{:S(2)}) async-start(), calls=%async_computation.8 | async-start | bytes 4792320 | tf_op jit(solution)/shard_map/all_gather | solution.py:37
  90.9 5.3 %all-to-all-start.4 = ((bf16[2,2048,44]{1,2,0:T(8,128)(2,1)}), bf16[2,2048,44]{1,2,0:T(8,128)(2,1)S(1)}, u32[]{:S(2)}, u32[]{:S(2)}) async-start(bf16[2,2048,44]{1,2,0:T(8,128)(2,1)} %pad_maximum_fusion), calls=%async_computation.4 | async-start | bytes 786432 | tf_op jit(solution)/shard_map/all_to_all | solution.py:48
  95.2 0.5 copy-start.17
  97.8 31.2 %all-to-all-start.1 = ((bf16[64,4,2048]{2,1,0:T(4,128)(2,1)}), bf16[64,4,2048]{2,1,0:T(4,128)(2,1)S(1)}, u32[]{:S(2)}, u32[]{:S(2)}) async-start(bf16[64,4,2048]{2,1,0:T(4,128)(2,1)} %bitcast.26), calls=%async_computation.1 | async-start | bytes 2097152 | tf_op jit(solution)/shard_map/all_to_all | solution.py:207
  133.2 34.8 %copy-start.6 = (bf16[1,2048,88]{1,2,0:T(8,128)(2,1)S(1)}, bf16[1,2048,88]{1,2,0:T(8,128)(2,1)}, u32[]{:S(2)}) copy-start(bf16[1,2048,88]{1,2,0:T(8,128)(2,1)} %all_to_all.41) | copy-start | bytes 1081348
  172.6 7.3 %all-to-all-start.6 = ((bf16[2,2048,88]{1,2,0:T(8,128)(2,1)}), bf16[2,2048,88]{1,2,0:T(8,128)(2,1)S(1)}, u32[]{:S(2)}, u32[]{:S(2)}) async-start(bf16[2,2048,88]{1,2,0:T(8,128)(2,1)} %broadcast_in_dim.43), calls=%async_computation.6 | async-start | bytes 1441792 | tf_op jit(solution)/shard_map/all_to_all | solution.py:16
  179.9 14.3 %copy-start.20 = (bf16[88,1024]{1,0:T(8,128)(2,1)S(1)}, bf16[88,1024]{1,0:T(8,128)(2,1)}, u32[]{:S(2)}) copy-start(bf16[88,1024]{1,0:T(8,128)(2,1)} %param.43) | copy-start | bytes 540676
  180.9 5.4 %all-to-all-start.5 = ((bf16[2,2048,88]{1,2,0:T(8,128)(2,1)}), bf16[2,2048,88]{1,2,0:T(8,128)(2,1)S(1)}, u32[]{:S(2)}, u32[]{:S(2)}) async-start(bf16[2,2048,88]{1,2,0:T(8,128)(2,1)} %broadcast_in_dim.42), calls=%async_computation.5 | async-start | bytes 1441792 | tf_op jit(solution)/shard_map/all_to_all | solution.py:16
  186.3 20.1 %all-to-all-start.3 = ((bf16[64,4,1024]{2,1,0:T(4,128)(2,1)}), bf16[64,4,1024]{2,1,0:T(4,128)(2,1)S(1)}, u32[]{:S(2)}, u32[]{:S(2)}) async-start(bf16[64,4,1024]{2,1,0:T(4,128)(2,1)} %copy.120), calls=%async_computation.3 | async-start | bytes 1048576 | tf_op jit(solution)/shard_map/all_to_all | solution.py:217
  206.4 5.8 %copy-start.18 = (s32[64]{0:T(128)S(1)}, s32[64]{0:T(128)}, u32[]{:S(2)}) copy-start(s32[64]{0:T(128)} %copy-done.17) | copy-start | bytes 772
  206.4 6.0 %copy-start.10 = (bf16[32,1,2,32]{3,2,0,1:T(2,128)(2,1)S(1)}, bf16[32,1,2,32]{3,2,0,1:T(2,128)(2,1)}, u32[]{:S(2)}) copy-start(bf16[32,1,2,32]{3,2,0,1:T(2,128)(2,1)} %copy-done.9) | copy-start | bytes 12292
  206.4 6.8 %copy-start.16 = (s32[32,2]{0,1:T(2,128)S(1)}, s32[32,2]{0,1:T(2,128)}, u32[]{:S(2)}) copy-start(s32[32,2]{0,1:T(2,128)} %param.35) | copy-start | bytes 772
  206.4 6.8 %copy-start.19 = (f32[32,2]{0,1:T(2,128)S(1)}, f32[32,2]{0,1:T(2,128)}, u32[]{:S(2)}) copy-start(f32[32,2]{0,1:T(2,128)} %param.36) | copy-start | bytes 772
  206.4 58.5 %all-to-all-start.7 = ((bf16[64,32,1024]{2,1,0:T(8,128)(2,1)}), bf16[64,32,1024]{2,1,0:T(8,128)(2,1)}, u32[]{:S(2)}, u32[]{:S(2)}) async-start(bf16[64,32,1024]{2,1,0:T(8,128)(2,1)} %bitcast.180), calls=%async_computation.7 | async-start | bytes 8388608 | tf_op jit(solution)/shard_map/all_to_all | solution.py:66
  212.3 55.7 %copy-start.3 = (f32[32,2048]{1,0:T(8,128)S(1)}, f32[32,2048]{1,0:T(8,128)}, u32[]{:S(2)}) copy-start(f32[32,2048]{1,0:T(8,128)} %get-tuple-element.141) | copy-start | bytes 786436
Sparse Core Ops, SparseCore 0:
  89.9 78.0 all-gather.1
where the time goes:
time: 278 us; the launch traced here: 276 us
  waiting for transfers between devices  108 us (39%)
  local copies, waits for them, and re-layouts  41.1 us (15%)
  matrix products  41.1 us (15%)
  starting transfers between devices  38 us (14%)
  other arithmetic  28 us (10%)
  between operations  15.3 us (6%)
  blocking collectives  4.14 us (1%)
    all_to_all x1, waiting for transfers between devices, sum_at_owner(): lax.all_to_all(pieces, axis, split_axis=0, concat_axis=0, tiled=True)  51.1 us
    all_gather x1, waiting for transfers between devices, in_one_piece(): filled, at, outs = (lax.all_gather(both, axis, axis=dim, tiled=True), 0, [])  28 us
    dynamic_slice x8, local copies, waits for them, and re-layouts, visit(): lax.dynamic_slice_in_dim(key_cache, offset, span_len, 1)  25.7 us
    all_to_all x1, waiting for transfers between devices, per_device(): lax.all_to_all(outgoing, 'ep', split_axis=0, concat_axis=0, tiled=True)  18.8 us
    all_to_all x1, starting transfers between devices, per_device(): lax.all_to_all(outgoing, 'ep', split_axis=0, concat_axis=0, tiled=True)  11.5 us
    dot_general x4, matrix products, visit(): jnp.einsum('sgaml,slge->sgame', weights.astype(jnp.bfloat16), cached, pre...  11.1 us
    all_to_all x3, starting transfers between devices, sent_to_all(): lax.all_to_all(jnp.broadcast_to(x[None], (size, *x.shape)), axis, 0, 0, t...  10.7 us
    all_to_all x1, waiting for transfers between devices, per_device(): lax.all_to_all(partial_value.astype(jnp.bfloat16), 'ep', split_axis=0, co...  7.86 us
  transfers between devices with their start and end apart: 8, of which 6 were waited for; matrix products, arithmetic and copies ran while one was open for 8% of the time, Pallas kernels for 0%

commit v1 on v0

--- a/solution.py
+++ b/solution.py
@@ -1,6 +1,8 @@
 import jax
 import jax.numpy as jnp
 from jax import lax
+from jax.experimental import pallas as pl
+from jax.experimental.pallas import tpu as pltpu
 from jax.sharding import PartitionSpec as P
 
 HEAD_DIM = 64
@@ -9,6 +11,123 @@
 
 norm_eps = 1e-05
 rope_base = 10000.0
+
+
+bf16=jnp.bfloat16; f32=jnp.float32
+ROWS=32; HEADS_L=8; CH=256; GRP=4
+
+def attention_body(lens, hid, gain, cos, sin, lam, hgain, wq_h, wk_h, wv_h, kc, vc, wo_h,
+                   part, nk, nv,
+                   wq, wk, wv, wo, kbuf, vbuf, qs, ks, vs, os_, wsem, ksem, vsem):
+    n_seq=hid.shape[0]; clen=kbuf.shape[1]
+    wcopies=[pltpu.make_async_copy(a,b,wsem.at[i]) for i,(a,b) in enumerate(((wq_h,wq),(wk_h,wk),(wv_h,wv),(wo_h,wo)))]
+    for c in wcopies[:3]: c.start()
+    def rows_of(s):
+        return pl.multiple_of(((lens[s]+15)//16)*16,16)
+    def kcopy(s):
+        n=rows_of(s)
+        return pltpu.make_async_copy(kc.at[s,pl.ds(0,n),:],kbuf.at[s,pl.ds(0,n),:],ksem.at[s])
+    def vcopy(s):
+        n=rows_of(s)
+        return pltpu.make_async_copy(vc.at[s,pl.ds(0,n),:],vbuf.at[s,pl.ds(0,n),:],vsem.at[s])
+    zero=jnp.zeros((clen,128),bf16)
+    def start(s,_):
+        vbuf[s]=zero
+        return 0
+    lax.fori_loop(0,n_seq,start,0)
+    def start2(s,_):
+        kcopy(s).start(); vcopy(s).start()
+        return 0
+    lax.fori_loop(0,n_seq,start2,0)
+    wcopies[3].start()
+    x=hid[...].astype(f32)
+    normed=(x*lax.rsqrt(jnp.mean(x*x,axis=-1,keepdims=True)+norm_eps)*gain[...]).astype(bf16)
+    lane=lax.broadcasted_iota(jnp.int32,(n_seq,128),1)
+    first=(lane%64)<32
+    c=cos[...]; sn=sin[...]
+    def rot(v):
+        other=jnp.where(first,pltpu.roll(v,96,1),pltpu.roll(v,32,1))
+        return (v*c+other*sn).astype(bf16)
+    wcopies[0].wait()
+    q=jnp.dot(normed,wq[...],preferred_element_type=f32)
+    for a in range(HEADS_L):
+        qs[pl.ds(a,n_seq,stride=HEADS_L),:]=rot(q[:,a*128:(a+1)*128]).astype(f32)
+    wcopies[1].wait(); wcopies[2].wait()
+    k=rot(jnp.dot(normed,wk[...],preferred_element_type=f32))
+    nk[...]=k; ks[...]=k.astype(f32)
+    v=jnp.dot(normed,wv[...],preferred_element_type=f32).astype(bf16)
+    nv[...]=v; vs[...]=v.astype(f32)
+    lane8=lax.broadcasted_iota(jnp.int32,(HEADS_L,128),1)
+    lamv=lam[...]; hg=hgain[...]
+    scale=64**-0.5
+    def one_group(g,C):
+        L=C*CH
+        sc=[];own=[]
+        for i in range(GRP):
+            s=g*GRP+i
+            kcopy(s).wait()
+            q8=qs[pl.ds(pl.multiple_of(s*8,8),8),:]
+            q16=jnp.concatenate([jnp.where(lane8<64,q8,0.0),jnp.where(lane8<64,0.0,q8)],axis=0)
+            own.append(jnp.sum(q16*ks[pl.ds(s,1),:],axis=-1,keepdims=True))
+            t=lax.dot_general(q16.astype(bf16),kbuf[s,0:L,:],(((1,),(1,)),((),())),preferred_element_type=f32)
+            pos=lax.broadcasted_iota(jnp.int32,(16,L),1)
+            sc.append(jnp.where(pos<lens[s],t,-jnp.inf))
+        for i in range(GRP):
+            s=g*GRP+i
+            m=jnp.maximum(jnp.max(sc[i],axis=-1,keepdims=True),own[i])
+            p=jnp.exp((sc[i]-m)*scale)
+            po=jnp.exp((own[i]-m)*scale)
+            tot=jnp.sum(p,axis=-1,keepdims=True)+po
+            vcopy(s).wait()
+            o=jnp.dot(p.astype(bf16),vbuf[s,0:L,:],preferred_element_type=f32)
+            o=o+po.astype(bf16).astype(f32)*vs[pl.ds(s,1),:]
+            o=o/tot
+            h=o[0:8]-lamv*o[8:16]
+            h=h*lax.rsqrt(jnp.mean(h*h,axis=-1,keepdims=True)+norm_eps)*hg
+            os_[pl.ds(pl.multiple_of(s*8,8),8),:]=h
+    def loop(g,_):
+        top=lens[g*GRP]
+        for i in range(1,GRP): top=jnp.maximum(top,lens[g*GRP+i])
+        need=(top+CH-1)//CH
+        for C in range(1,clen//CH+1):
+            @pl.when(need==C)
+            def _(): one_group(g,C)
+        return 0
+    lax.fori_loop(0,n_seq//GRP,loop,0)
+    ho=jnp.concatenate([os_[pl.ds(a,n_seq,stride=HEADS_L),:] for a in range(HEADS_L)],axis=-1).astype(bf16)
+    wcopies[3].wait()
+    part[...]=jnp.dot(ho,wo[...],preferred_element_type=f32).astype(bf16)
+
+def attention(past_lengths,hidden_in,attn_gain,w_query,w_key,w_value,key_cache,value_cache,lambdas,head_gain,w_out):
+    n,d=hidden_in.shape; clen=key_cache.shape[1]
+    mid=32
+    inv=10000.0**(-jnp.arange(mid,dtype=f32)/mid)
+    ang=past_lengths.astype(f32)[:,None]*inv[None,:]
+    co=jnp.cos(ang); si=jnp.sin(ang)
+    cos=jnp.concatenate([co,co,co,co],-1); sin=jnp.concatenate([-si,si,-si,si],-1)
+    vm=pl.BlockSpec(memory_space=pltpu.VMEM); an=pl.BlockSpec(memory_space=pltpu.HBM); sm=pl.BlockSpec(memory_space=pltpu.SMEM)
+    return pl.pallas_call(attention_body,
+        out_shape=(jax.ShapeDtypeStruct((n,w_out.shape[1]),bf16),jax.ShapeDtypeStruct((n,128),bf16),jax.ShapeDtypeStruct((n,128),bf16)),
+        in_specs=[sm]+[vm]*6+[an]*6,
+        out_specs=(vm,vm,vm),
+        scratch_shapes=[pltpu.VMEM(w_query.shape,bf16),pltpu.VMEM(w_key.shape,bf16),pltpu.VMEM(w_value.shape,bf16),pltpu.VMEM(w_out.shape,bf16),
+            pltpu.VMEM(key_cache.shape,bf16),pltpu.VMEM(value_cache.shape,bf16),
+            pltpu.VMEM((n*8,128),f32),pltpu.VMEM((n,128),f32),pltpu.VMEM((n,128),f32),pltpu.VMEM((n*8,128),f32),
+            pltpu.SemaphoreType.DMA((4,)),pltpu.SemaphoreType.DMA((n,)),pltpu.SemaphoreType.DMA((n,))],
+        compiler_params=pltpu.CompilerParams(vmem_limit_bytes=62*1024*1024),
+        name="attention",
+    )(past_lengths,hidden_in,attn_gain.reshape(1,-1),cos,sin,lambdas.reshape(-1,1),head_gain.reshape(1,-1),w_query,w_key,w_value,key_cache,value_cache,w_out)
+
+
+def swapped(x):
+    return lax.ppermute(x, "tp", [(0, 1), (1, 0)])
+
+
+def both_cores(x, rank):
+    other = swapped(x)
+    first = jnp.where(rank == 0, x, other)
+    second = jnp.where(rank == 0, other, x)
+    return jnp.concatenate([first, second], axis=1)
 
 
 def sent_to_all(x, axis):
@@ -16,8 +135,8 @@
     return lax.all_to_all(jnp.broadcast_to(x[None], (size, *x.shape)), axis, 0, 0, tiled=True)
 
 
-def taken_together(x, axis):
-    return sent_to_all(x, axis).astype(jnp.float32).sum(axis=0)
+def taken_together(x):
+    return x.astype(jnp.float32) + swapped(x).astype(jnp.float32)
 
 
 def in_order(pieces, dim):
@@ -113,77 +232,13 @@
     ep_count = lax.axis_size("ep")
     tp_rank = lax.axis_index("tp")
     half_width = model_width // tp_count
-    heads_here = lambdas.shape[0]
-    kv_here = w_key.shape[1] // (2 * HEAD_DIM)
-    per_key = heads_here // kv_here
-    scale_qk = HEAD_DIM ** (-0.5)
-    normed = rms_rows(hidden_in, attn_gain).astype(jnp.bfloat16)
-    queries = rotary(
-        jnp.dot(normed, w_query, preferred_element_type=jnp.float32).reshape(
-            batch_rows, heads_here, 2, HEAD_DIM
-        ),
-        past_lengths,
+    own_part, key_new, value_new = attention(
+        past_lengths, hidden_in, attn_gain, w_query, w_key, w_value, key_cache, value_cache,
+        lambdas, head_gain, w_out,
+    )
+    attn_out = (
+        own_part.astype(jnp.float32) + swapped(own_part).astype(jnp.float32)
     ).astype(jnp.bfloat16)
-    key_new = rotary(
-        jnp.dot(normed, w_key, preferred_element_type=jnp.float32).reshape(
-            batch_rows, kv_here, 2, HEAD_DIM
-        ),
-        past_lengths,
-    ).astype(jnp.bfloat16)
-    value_new = jnp.dot(normed, w_value, preferred_element_type=jnp.float32).astype(jnp.bfloat16)
-    grouped = queries.reshape(batch_rows, kv_here, per_key, 2, HEAD_DIM)
-    own_score = (
-        jnp.einsum("sgamd,sgmd->sgam", grouped, key_new, preferred_element_type=jnp.float32)
-        * scale_qk
-    )
-    value_rows = value_new.reshape(batch_rows, kv_here, 1, 1, VALUE_DIM).astype(jnp.float32)
-    start_state = (
-        own_score,
-        jnp.ones_like(own_score),
-        jnp.broadcast_to(value_rows, own_score.shape + (VALUE_DIM,)),
-    )
-    cache_len = key_cache.shape[1]
-    span_len = min(256, cache_len)
-    spans_needed = (jnp.max(past_lengths) + span_len - 1) // span_len
-
-    def visit(block_index, carried):
-        running, totals, summed = carried
-        offset = block_index * span_len
-        key_rows = lax.dynamic_slice_in_dim(key_cache, offset, span_len, 1).reshape(
-            batch_rows, span_len, kv_here, 2, HEAD_DIM
-        )
-        cached = lax.dynamic_slice_in_dim(value_cache, offset, span_len, 1).reshape(
-            batch_rows, span_len, kv_here, VALUE_DIM
-        )
-        scores = (
-            jnp.einsum("sgamd,slgmd->sgaml", grouped, key_rows, preferred_element_type=jnp.float32)
-            * scale_qk
-        )
-        usable = (offset + jnp.arange(span_len))[None, :] < past_lengths[:, None]
-        scores = jnp.where(usable[:, None, None, None, :], scores, -jnp.inf)
-        raised = jnp.maximum(running, jnp.max(scores, axis=-1))
-        fading = jnp.exp(running - raised)
-        weights = jnp.exp(scores - raised[..., None])
-        totals = totals * fading + jnp.sum(weights, axis=-1)
-        summed = summed * fading[..., None] + jnp.einsum(
-            "sgaml,slge->sgame",
-            weights.astype(jnp.bfloat16),
-            cached,
-            preferred_element_type=jnp.float32,
-        )
-        return (raised, totals, summed)
-
-    running, totals, summed = lax.fori_loop(0, spans_needed, visit, start_state)
-    mapped = summed / totals[..., None]
-    head_mix = mapped[..., 0, :] - lambdas.reshape(1, kv_here, per_key, 1) * mapped[..., 1, :]
-    head_out = rms_rows(head_mix, head_gain).astype(jnp.bfloat16).reshape(batch_rows, -1)
-    attn_out = (
-        taken_together(
-            jnp.dot(head_out, w_out, preferred_element_type=jnp.float32).astype(jnp.bfloat16), "tp"
-        )
-        .astype(jnp.float32)
-        .astype(jnp.bfloat16)
-    )
     residual = hidden_in.astype(jnp.float32) + attn_out.astype(jnp.float32)
     moe_in = rms_rows(residual, ffn_gain).astype(jnp.bfloat16)
     mix_gate = jax.nn.sigmoid(
@@ -210,7 +265,7 @@
     gate_pre = jnp.dot(flat_rows, expert_gate[0], preferred_element_type=jnp.float32)
     up_pre = jnp.dot(flat_rows, expert_up[0], preferred_element_type=jnp.float32)
     inner_act = (jax.nn.silu(gate_pre) * up_pre).astype(jnp.bfloat16)
-    inner_act = collect(inner_act, "tp", 1)
+    inner_act = both_cores(inner_act, tp_rank)
     partial_value = jnp.dot(inner_act, expert_down[0], preferred_element_type=jnp.float32).reshape(
         leading + (half_width,)
     )
@@ -244,12 +299,10 @@
             jnp.dot(rows_all, gate_cols[0], preferred_element_type=jnp.float32).astype(
                 jnp.bfloat16
             ),
-            "tp",
-        ).astype(jnp.float32),
+        ),
         taken_together(
             jnp.dot(rows_all, up_cols[0], preferred_element_type=jnp.float32).astype(jnp.bfloat16),
-            "tp",
-        ).astype(jnp.float32),
+        ),
     )
     dense_act = (jax.nn.silu(pre_gate) * pre_up).astype(jnp.bfloat16)
     gate_rows = gates_all.astype(jnp.float32)

time: 278 us -> 211 us (0.76)
  local copies, waits for them, and re-layouts: 41.1 us -> 8.2 us
  matrix products: 41.1 us -> 16.2 us
  Pallas kernels: 0 us -> 18.8 us
  other arithmetic: 28 us -> 9.33 us
  starting transfers between devices: 38 us -> 29.4 us
  waiting for transfers between devices: 108 us -> 114 us
  blocking collectives: 4.14 us -> 0 us
    dynamic_slice x8 -> x0, local copies, waits for them, and re-layouts: 25.7 us -> none  [visit(): lax.dynamic_slice_in_dim(key_cache, offset, span_len, 1)]
    dot_general x13 -> x0, matrix products: 23.6 us -> none  [the longest x4 11.1 us: visit(): jnp.einsum('sgaml,slge->sgame', weights.astype(jnp.bfloat16), cached, pre...]
    pallas_call x0 -> x1, Pallas kernels: none -> 18.8 us  [attention(): pl.pallas_call(attention_body, out_shape=(jax.ShapeDtypeStruct((n, w_out....]
    all_to_all x3 -> x0, starting transfers between devices: 10.7 us -> none  [sent_to_all(): lax.all_to_all(jnp.broadcast_to(x[None], (size, *x.shape)), axis, 0, 0, t...]
    add x9 -> x0, other arithmetic: 6.59 us -> none  [the longest x4 5.71 us: visit(): totals = totals * fading + jnp.sum(weights, axis=-1)]
    all_gather x1, waiting for transfers between devices: 28 us -> 32.6 us  [in_one_piece(): filled, at, outs = (lax.all_gather(both, axis, axis=dim, tiled=True), 0, [])]
    all_to_all x1 -> x0, blocking collectives: 4.14 us -> none  [sent_to_all(): lax.all_to_all(jnp.broadcast_to(x[None], (size, *x.shape)), axis, 0, 0, t...]
    broadcast_in_dim x6 -> x0, local copies, waits for them, and re-layouts: 4.03 us -> none  [the longest x4 2.69 us: sent_to_all(): jnp.broadcast_to(x[None], (size, *x.shape))]
  transfers between devices with their start and end apart: 8 -> 9, of which waited for: 6 -> 6; matrix products, arithmetic and copies ran while one was open for 8% -> 10% of each run, Pallas kernels for 0% -> 0%
where the time goes in v1:
time: 211 us; the launch traced here: 210 us
  waiting for transfers between devices  114 us (54%)
  starting transfers between devices  29.4 us (14%)
  Pallas kernels  18.8 us (9%)
  matrix products  16.2 us (8%)
  between operations  14.4 us (7%)
  other arithmetic  9.33 us (4%)
  local copies, waits for them, and re-layouts  8.2 us (4%)
    all_to_all x1, waiting for transfers between devices, sum_at_owner(): lax.all_to_all(pieces, axis, split_axis=0, concat_axis=0, tiled=True)  51.9 us
    all_gather x1, waiting for transfers between devices, in_one_piece(): filled, at, outs = (lax.all_gather(both, axis, axis=dim, tiled=True), 0, [])  32.6 us
    pallas_call x1, Pallas kernels, attention(): pl.pallas_call(attention_body, out_shape=(jax.ShapeDtypeStruct((n, w_out....  18.8 us
    all_to_all x1, waiting for transfers between devices, per_device(): lax.all_to_all(outgoing, 'ep', split_axis=0, concat_axis=0, tiled=True)  18.2 us
    all_to_all x1, starting transfers between devices, per_device(): lax.all_to_all(outgoing, 'ep', split_axis=0, concat_axis=0, tiled=True)  12.9 us
    all_to_all x1, waiting for transfers between devices, per_device(): lax.all_to_all(partial_value.astype(jnp.bfloat16), 'ep', split_axis=0, co...  7.91 us
    all_to_all x1, starting transfers between devices, per_device(): lax.all_to_all(partial_value.astype(jnp.bfloat16), 'ep', split_axis=0, co...  6.46 us
    all_to_all x1, starting transfers between devices, sum_at_owner(): lax.all_to_all(pieces, axis, split_axis=0, concat_axis=0, tiled=True)  5.79 us
  transfers between devices with their start and end apart: 9, of which 6 were waited for; matrix products, arithmetic and copies ran while one was open for 10% of the time, Pallas kernels for 0%

profile of v1, /device:TPU:0, one launch (start us, length us, event | category | flops | bytes accessed | tf_op | source)
XLA Modules:
  0.0 210.2 jit_solution(2055416039145656943)
XLA Ops:
  7.2 0.8 convert_element_type.76
  8.0 1.3 copy.79.lam
  9.3 0.1 fusion.37
  9.5 0.7 pad_maximum_fusion.3
  10.2 18.8 %attention.1 = (bf16[32,2048]{1,0:T(8,128)(2,1)}, bf16[32,128]{1,0:T(8,128)(2,1)}, bf16[32,128]{1,0:T(8,128)(2,1)}) custom-call(s32[32]{0:T(128)} %lens.1, bf16[32,2048]{1,0:T(8,128)(2,1)} %hid.1, f32[1,2048]{1,0:T(1,128)} %bitcast.65, f32[32,128]{1,0:T(8,128)} %get-tuple-element.16.cos, f32[32,128]{1,0:T(8,128)} %get-tuple-element.17.sin, ...), custom_call_target="tpu_custom_call" | custom-call | tf_op jit(solution)/shard_map/attention/pallas_call | solution.py:109
  29.2 1.5 collective-permute-done
  30.7 1.1 multiply_reduce_fusion
  31.8 0.7 copy-done.1
  32.6 0.1 fusion.32
  32.7 0.1 copy.87
  32.9 0.6 pad_maximum_fusion.2
  33.6 0.1 eq.40
  33.8 0.1 reduce_window_sum.11
  33.9 0.2 select_reduce_fusion.1
  34.1 0.2 broadcast_in_dim.6
  34.3 0.1 reshape.96
  34.4 0.3 convolution_convert_fusion
  34.7 0.2 broadcast_in_dim.7
  34.9 1.6 broadcast_in_dim.8
  36.4 12.9 %all-to-all-start = ((bf16[64,4,2048]{2,1,0:T(4,128)(2,1)}), bf16[64,4,2048]{2,1,0:T(4,128)(2,1)S(1)}, u32[]{:S(2)}, u32[]{:S(2)}) async-start(bf16[64,4,2048]{2,1,0:T(4,128)(2,1)} %bitcast.3), calls=%async_computation | async-start | bytes 2097152 | tf_op jit(solution)/shard_map/all_to_all | solution.py:262
  49.4 0.1 reshape.104
  49.5 0.7 copy.89
  50.3 0.7 copy.88
  51.0 18.2 %all-to-all-done = bf16[64,4,2048]{2,1,0:T(4,128)(2,1)S(1)} async-done(((bf16[64,4,2048]{2,1,0:T(4,128)(2,1)}), bf16[64,4,2048]{2,1,0:T(4,128)(2,1)S(1)}, u32[]{:S(2)}, u32[]{:S(2)}) %all-to-all-start) | async-done | bytes 1048608 | tf_op jit(solution)/shard_map/all_to_all | solution.py:262
  69.2 0.3 reshape.98
  69.5 2.0 fusion.14
  71.5 1.9 fusion.22
  73.5 0.8 pad_maximum_fusion
  74.3 3.5 %all-to-all-start.2 = ((bf16[2,2048,44]{1,2,0:T(8,128)(2,1)}), bf16[2,2048,44]{1,2,0:T(8,128)(2,1)S(1)}, u32[]{:S(2)}, u32[]{:S(2)}) async-start(bf16[2,2048,44]{1,2,0:T(8,128)(2,1)} %pad_maximum_fusion), calls=%async_computation.2 | async-start | bytes 786432 | tf_op jit(solution)/shard_map/all_to_all | solution.py:167
  77.8 1.6 all-to-all-done.2
  79.6 0.2 copy.82
  79.8 0.1 dot_general.32
  79.9 32.6 %all-gather.2.cloned.1.call-done = bf16[2048,1025]{1,0:T(8,128)(2,1)} async-done(((bf16[32,1025]{1,0:T(8,128)(2,1)}), bf16[2048,1025]{1,0:T(8,128)(2,1)}) %all-gather.2.cloned.1.call-update) | async-done | bytes 4198416 | tf_op jit(solution)/shard_map/all_gather | solution.py:156
  112.5 3.7 %fusion.7 = bf16[2048,88]{0,1:T(8,128)(2,1)S(1)} fusion(bf16[2048,1025]{1,0:T(8,128)(2,1)} %all-gather.2.cloned.1.call-done, bf16[1,2048,88]{1,2,0:T(8,128)(2,1)S(1)} %all_to_all.27), kind=kOutput, calls=%fused_computation.8 | convolution fusion | flops 369278976 | bytes 4734976 | tf_op jit(solution)/shard_map/dot_general | solution.py:304
  116.3 2.2 %fusion.4 = bf16[2048,88]{0,1:T(8,128)(2,1)} fusion(bf16[2048,1025]{1,0:T(8,128)(2,1)S(1)} %copy-done.8, bf16[1,2048,88]{1,2,0:T(8,128)(2,1)S(1)} %all_to_all.27), kind=kOutput, calls=%fused_computation.7 | convolution fusion | flops 369278976 | bytes 4734976 | tf_op jit(solution)/shard_map/dot_general | solution.py:299
  118.5 0.5 collective-permute-start.2
  119.0 0.6 fusion.16
  119.6 1.2 copy.84
  120.8 6.5 %all-to-all-start.1 = ((bf16[64,4,1024]{2,1,0:T(4,128)(2,1)}), bf16[64,4,1024]{2,1,0:T(4,128)(2,1)S(1)}, u32[]{:S(2)}, u32[]{:S(2)}) async-start(bf16[64,4,1024]{2,1,0:T(4,128)(2,1)} %copy.84), calls=%async_computation.1 | async-start | bytes 1048576 | tf_op jit(solution)/shard_map/all_to_all | solution.py:272
  127.2 1.3 convert_reduce_fusion.2
  128.5 4.4 %multiply_convert_fusion = bf16[2048,1024]{1,0:T(8,128)(2,1)} fusion(bf16[88,1024]{1,0:T(8,128)(2,1)S(1)} %copy-done.13, f32[2048]{0:T(1024)S(1)} %convert_reduce_fusion.2, bf16[2048,88]{0,1:T(8,128)(2,1)S(1)} %collective-permute-done.3, bf16[2048,88]{0,1:T(8,128)(2,1)S(1)} %fusion.7, bf16[2048,88]{0,1:T(8,128)(2,1)S(1)} %collective-permute-done.2, ...), kind=kOutput, calls=%fused_computation.1 | convolution fusion | flops 375455744 | bytes 5824512 | tf_op jit(solution)/shard_map/dot_general | solution.py:311
  132.9 7.9 %all-to-all-done.1 = bf16[64,4,1024]{2,1,0:T(4,128)(2,1)S(1)} async-done(((bf16[64,4,1024]{2,1,0:T(4,128)(2,1)}), bf16[64,4,1024]{2,1,0:T(4,128)(2,1)S(1)}, u32[]{:S(2)}, u32[]{:S(2)}) %all-to-all-start.1) | async-done | bytes 524320 | tf_op jit(solution)/shard_map/all_to_all | solution.py:272
  140.8 5.8 %all-to-all-start.3 = ((bf16[64,32,1024]{2,1,0:T(8,128)(2,1)}), bf16[64,32,1024]{2,1,0:T(8,128)(2,1)}, u32[]{:S(2)}, u32[]{:S(2)}) async-start(bf16[64,32,1024]{2,1,0:T(8,128)(2,1)} %bitcast.63), calls=%async_computation.3 | async-start | bytes 8388608 | tf_op jit(solution)/shard_map/all_to_all | solution.py:185
  146.9 0.3 convert_reduce_fusion.1
  147.2 0.2 reshape.101
  147.4 51.9 %all-to-all-done.3 = bf16[64,32,1024]{2,1,0:T(8,128)(2,1)} async-done(((bf16[64,32,1024]{2,1,0:T(8,128)(2,1)}), bf16[64,32,1024]{2,1,0:T(8,128)(2,1)}, u32[]{:S(2)}, u32[]{:S(2)}) %all-to-all-start.3) | async-done | bytes 4194336 | tf_op jit(solution)/shard_map/all_to_all | solution.py:185
  199.3 3.0 %convert_reduce_fusion = f32[32,1024]{1,0:T(8,128)S(1)} fusion(bf16[64,32,1024]{2,1,0:T(8,128)(2,1)} %all-to-all-done.3), kind=kLoop, calls=%fused_computation | loop fusion | flops 4161536 | bytes 4325376 | tf_op jit(solution)/shard_map/reduce_sum | solution.py:186
  202.3 1.0 fusion.26
  (51 shorter events, 1.2 us)
Async XLA Ops:
  7.2 111.8 %copy-start = (bf16[1,704,1024]{2,1,0:T(8,128)(2,1)S(1)}, bf16[1,704,1024]{2,1,0:T(8,128)(2,1)}, u32[]{:S(2)}) copy-start(bf16[1,704,1024]{2,1,0:T(8,128)(2,1)} %param.37) | copy-start | bytes 4325380
  7.2 105.3 %all-gather.2.cloned.1.call-start = ((), (), s32[]{:S(2)}) async-start(), calls=%async_computation.4 | async-start | bytes 4792320 | tf_op jit(solution)/shard_map/all_gather | solution.py:156
  10.2 19.0 %copy-start.10 = (bf16[2048]{0:T(1024)(128)(2,1)S(1)}, bf16[2048]{0:T(1024)(128)(2,1)}, u32[]{:S(2)}) copy-start(bf16[2048]{0:T(1024)(128)(2,1)} %param.38) | copy-start | bytes 12292
  10.2 20.5 %copy-start.5 = (bf16[32,2048]{1,0:T(8,128)(2,1)S(1)}, bf16[32,2048]{1,0:T(8,128)(2,1)}, u32[]{:S(2)}) copy-start(bf16[32,2048]{1,0:T(8,128)(2,1)} %hid.1) | copy-start | bytes 393220
  10.2 22.3 %copy-start.9 = (f32[2048]{0:T(1024)S(1)}, f32[2048]{0:T(1024)}, u32[]{:S(2)}) copy-start(f32[2048]{0:T(1024)} %param.32) | copy-start | bytes 24580
  10.2 23.3 %copy-start.11 = (s32[32,2]{0,1:T(2,128)S(1)}, s32[32,2]{0,1:T(2,128)}, u32[]{:S(2)}) copy-start(s32[32,2]{0,1:T(2,128)} %param.33) | copy-start | bytes 772
  29.0 20.3 %copy-start.6 = (bf16[2048,44]{0,1:T(8,128)(2,1)S(1)}, bf16[2048,44]{0,1:T(8,128)(2,1)}, u32[]{:S(2)}) copy-start(bf16[2048,44]{0,1:T(8,128)(2,1)} %param.40) | copy-start | bytes 540676
  29.0 1.6 collective-permute-start
  31.8 0.7 copy-start.1
  31.8 18.4 %copy-start.7 = (bf16[2048,44]{0,1:T(8,128)(2,1)S(1)}, bf16[2048,44]{0,1:T(8,128)(2,1)}, u32[]{:S(2)}) copy-start(bf16[2048,44]{0,1:T(8,128)(2,1)} %param.39) | copy-start | bytes 540676
  36.4 32.8 %all-to-all-start = ((bf16[64,4,2048]{2,1,0:T(4,128)(2,1)}), bf16[64,4,2048]{2,1,0:T(4,128)(2,1)S(1)}, u32[]{:S(2)}, u32[]{:S(2)}) async-start(bf16[64,4,2048]{2,1,0:T(4,128)(2,1)} %bitcast.3), calls=%async_computation | async-start | bytes 2097152 | tf_op jit(solution)/shard_map/all_to_all | solution.py:262
  69.5 4.1 %copy-start.3 = (bf16[2,1024,44]{1,2,0:T(8,128)(2,1)S(1)}, bf16[2,1024,44]{1,2,0:T(8,128)(2,1)}, u32[]{:S(2)}) copy-start(bf16[2,1024,44]{1,2,0:T(8,128)(2,1)} %copy.89) | copy-start | bytes 540676
  69.5 4.1 %copy-start.4 = (bf16[2,1024,44]{1,2,0:T(8,128)(2,1)S(1)}, bf16[2,1024,44]{1,2,0:T(8,128)(2,1)}, u32[]{:S(2)}) copy-start(bf16[2,1024,44]{1,2,0:T(8,128)(2,1)} %copy.88) | copy-start | bytes 540676
  73.4 6.1 %collective-permute-start.1 = (bf16[256,352]{0,1:T(8,128)(2,1)S(1)}, bf16[256,352]{0,1:T(8,128)(2,1)S(1)}, u32[]{:S(2)}, u32[]{:S(2)}) collective-permute-start(bf16[256,352]{0,1:T(8,128)(2,1)S(1)} %fusion.22), channel_id=1, source_target_pairs={{0,1},{1,0},{2,3},{3,2},{4,5},{5,4},{6,7},{7,6},{8,9},{9,8},{10,11... | collective-permute-start | bytes 540680 | tf_op jit(solution)/shard_map/ppermute | solution.py:123
  74.3 5.1 %all-to-all-start.2 = ((bf16[2,2048,44]{1,2,0:T(8,128)(2,1)}), bf16[2,2048,44]{1,2,0:T(8,128)(2,1)S(1)}, u32[]{:S(2)}, u32[]{:S(2)}) async-start(bf16[2,2048,44]{1,2,0:T(8,128)(2,1)} %pad_maximum_fusion), calls=%async_computation.2 | async-start | bytes 786432 | tf_op jit(solution)/shard_map/all_to_all | solution.py:167
  112.5 3.8 %copy-start.8 = (bf16[2048,1025]{1,0:T(8,128)(2,1)S(1)}, bf16[2048,1025]{1,0:T(8,128)(2,1)}, u32[]{:S(2)}) copy-start(bf16[2048,1025]{1,0:T(8,128)(2,1)} %all-gather.2.cloned.1.call-done) | copy-start | bytes 12595204
  116.2 12.3 %collective-permute-start.3 = (bf16[2048,88]{0,1:T(8,128)(2,1)S(1)}, bf16[2048,88]{0,1:T(8,128)(2,1)S(1)}, u32[]{:S(2)}, u32[]{:S(2)}) collective-permute-start(bf16[2048,88]{0,1:T(8,128)(2,1)S(1)} %fusion.7), channel_id=1, source_target_pairs={{0,1},{1,0},{2,3},{3,2},{4,5},{5,4},{6,7},{7,6},{8,9},{9,8},{10,11... | collective-permute-start | bytes 1081352 | tf_op jit(solution)/shard_map/ppermute | solution.py:123
  118.5 10.0 %copy-start.13 = (bf16[88,1024]{1,0:T(8,128)(2,1)S(1)}, bf16[88,1024]{1,0:T(8,128)(2,1)}, u32[]{:S(2)}) copy-start(bf16[88,1024]{1,0:T(8,128)(2,1)} %param.41) | copy-start | bytes 540676
  118.5 10.0 %collective-permute-start.2 = (bf16[2048,88]{0,1:T(8,128)(2,1)}, bf16[2048,88]{0,1:T(8,128)(2,1)S(1)}, u32[]{:S(2)}, u32[]{:S(2)}) collective-permute-start(bf16[2048,88]{0,1:T(8,128)(2,1)} %fusion.4), channel_id=1, source_target_pairs={{0,1},{1,0},{2,3},{3,2},{4,5},{5,4},{6,7},{7,6},{8,9},{9,8},{10,11... | collective-permute-start | bytes 1081352 | tf_op jit(solution)/shard_map/ppermute | solution.py:123
  120.8 20.0 %all-to-all-start.1 = ((bf16[64,4,1024]{2,1,0:T(4,128)(2,1)}), bf16[64,4,1024]{2,1,0:T(4,128)(2,1)S(1)}, u32[]{:S(2)}, u32[]{:S(2)}) async-start(bf16[64,4,1024]{2,1,0:T(4,128)(2,1)} %copy.84), calls=%async_computation.1 | async-start | bytes 1048576 | tf_op jit(solution)/shard_map/all_to_all | solution.py:272
  140.8 6.0 %copy-start.12 = (f32[32,2]{0,1:T(2,128)S(1)}, f32[32,2]{0,1:T(2,128)}, u32[]{:S(2)}) copy-start(f32[32,2]{0,1:T(2,128)} %param.34) | copy-start | bytes 772
  140.8 58.5 %all-to-all-start.3 = ((bf16[64,32,1024]{2,1,0:T(8,128)(2,1)}), bf16[64,32,1024]{2,1,0:T(8,128)(2,1)}, u32[]{:S(2)}, u32[]{:S(2)}) async-start(bf16[64,32,1024]{2,1,0:T(8,128)(2,1)} %bitcast.63), calls=%async_computation.3 | async-start | bytes 8388608 | tf_op jit(solution)/shard_map/all_to_all | solution.py:185
  146.6 55.7 %copy-start.2 = (f32[32,2048]{1,0:T(8,128)S(1)}, f32[32,2048]{1,0:T(8,128)}, u32[]{:S(2)}) copy-start(f32[32,2048]{1,0:T(8,128)} %copy-done.1) | copy-start | bytes 786436
Sparse Core Ops, SparseCore 0:
  33.6 78.7 all-gather.1

commit v2 on v1

v2 whole, which is shorter than its diff:
```python
import jax
import jax.numpy as jnp
from jax import lax
from jax.experimental import pallas as pl
from jax.experimental.pallas import tpu as pltpu
from jax.sharding import PartitionSpec as P

bf16=jnp.bfloat16; f32=jnp.float32
norm_eps=1e-05
ROWS=32; HEADS_L=8; CH=256; GRP=4

def attention_body(lens, hid, gain, cos, sin, lam, hgain, wq_h, wk_h, wv_h, kc, vc, wo_h,
                   part, nk, nv,
                   wq, wk, wv, wo, kbuf, vbuf, qs, ks, vs, os_, wsem, ksem, vsem):
    n_seq=hid.shape[0]; clen=kbuf.shape[1]
    wcopies=[pltpu.make_async_copy(a,b,wsem.at[i]) for i,(a,b) in enumerate(((wq_h,wq),(wk_h,wk),(wv_h,wv),(wo_h,wo)))]
    for c in wcopies[:3]: c.start()
    def rows_of(s):
        return pl.multiple_of(((lens[s]+15)//16)*16,16)
    def kcopy(s):
        n=rows_of(s)
        return pltpu.make_async_copy(kc.at[s,pl.ds(0,n),:],kbuf.at[s,pl.ds(0,n),:],ksem.at[s])
    def vcopy(s):
        n=rows_of(s)
        return pltpu.make_async_copy(vc.at[s,pl.ds(0,n),:],vbuf.at[s,pl.ds(0,n),:],vsem.at[s])
    zero=jnp.zeros((clen,128),bf16)
    def start(s,_):
        vbuf[s]=zero
        return 0
    lax.fori_loop(0,n_seq,start,0)
    def start2(s,_):
        kcopy(s).start(); vcopy(s).start()
        return 0
    lax.fori_loop(0,n_seq,start2,0)
    wcopies[3].start()
    x=hid[...].astype(f32)
    normed=(x*lax.rsqrt(jnp.mean(x*x,axis=-1,keepdims=True)+norm_eps)*gain[...]).astype(bf16)
    lane=lax.broadcasted_iota(jnp.int32,(n_seq,128),1)
    first=(lane%64)<32
    c=cos[...]; sn=sin[...]
    def rot(v):
        other=jnp.where(first,pltpu.roll(v,96,1),pltpu.roll(v,32,1))
        return (v*c+other*sn).astype(bf16)
    wcopies[0].wait()
    q=jnp.dot(normed,wq[...],preferred_element_type=f32)
    for a in range(HEADS_L):
        qs[pl.ds(a,n_seq,stride=HEADS_L),:]=rot(q[:,a*128:(a+1)*128]).astype(f32)
    wcopies[1].wait(); wcopies[2].wait()
    k=rot(jnp.dot(normed,wk[...],preferred_element_type=f32))
    nk[...]=k; ks[...]=k.astype(f32)
    v=jnp.dot(normed,wv[...],preferred_element_type=f32).astype(bf16)
    nv[...]=v; vs[...]=v.astype(f32)
    lane8=lax.broadcasted_iota(jnp.int32,(HEADS_L,128),1)
    lamv=lam[...]; hg=hgain[...]
    scale=64**-0.5
    def one_group(g,C):
        L=C*CH
        sc=[];own=[]
        for i in range(GRP):
            s=g*GRP+i
            kcopy(s).wait()
            q8=qs[pl.ds(pl.multiple_of(s*8,8),8),:]
            q16=jnp.concatenate([jnp.where(lane8<64,q8,0.0),jnp.where(lane8<64,0.0,q8)],axis=0)
            own.append(jnp.sum(q16*ks[pl.ds(s,1),:],axis=-1,keepdims=True))
            t=lax.dot_general(q16.astype(bf16),kbuf[s,0:L,:],(((1,),(1,)),((),())),preferred_element_type=f32)
            pos=lax.broadcasted_iota(jnp.int32,(16,L),1)
            sc.append(jnp.where(pos<lens[s],t,-jnp.inf))
        for i in range(GRP):
            s=g*GRP+i
            m=jnp.maximum(jnp.max(sc[i],axis=-1,keepdims=True),own[i])
            p=jnp.exp((sc[i]-m)*scale)
            po=jnp.exp((own[i]-m)*scale)
            tot=jnp.sum(p,axis=-1,keepdims=True)+po
            vcopy(s).wait()
            o=jnp.dot(p.astype(bf16),vbuf[s,0:L,:],preferred_element_type=f32)
            o=o+po.astype(bf16).astype(f32)*vs[pl.ds(s,1),:]
            o=o/tot
            h=o[0:8]-lamv*o[8:16]
            h=h*lax.rsqrt(jnp.mean(h*h,axis=-1,keepdims=True)+norm_eps)*hg
            os_[pl.ds(pl.multiple_of(s*8,8),8),:]=h
    def loop(g,_):
        top=lens[g*GRP]
        for i in range(1,GRP): top=jnp.maximum(top,lens[g*GRP+i])
        need=(top+CH-1)//CH
        for C in range(1,clen//CH+1):
            @pl.when(need==C)
            def _(): one_group(g,C)
        return 0
    lax.fori_loop(0,n_seq//GRP,loop,0)
    ho=jnp.concatenate([os_[pl.ds(a,n_seq,stride=HEADS_L),:] for a in range(HEADS_L)],axis=-1).astype(bf16)
    wcopies[3].wait()
    part[...]=jnp.dot(ho,wo[...],preferred_element_type=f32).astype(bf16)

def attention(past_lengths,hidden_in,attn_gain,w_query,w_key,w_value,key_cache,value_cache,lambdas,head_gain,w_out):
    n,d=hidden_in.shape; clen=key_cache.shape[1]
    mid=32
    inv=10000.0**(-jnp.arange(mid,dtype=f32)/mid)
    ang=past_lengths.astype(f32)[:,None]*inv[None,:]
    co=jnp.cos(ang); si=jnp.sin(ang)
    cos=jnp.concatenate([co,co,co,co],-1); sin=jnp.concatenate([-si,si,-si,si],-1)
    vm=pl.BlockSpec(memory_space=pltpu.VMEM); an=pl.BlockSpec(memory_space=pltpu.HBM); sm=pl.BlockSpec(memory_space=pltpu.SMEM)
    return pl.pallas_call(attention_body,
        out_shape=(jax.ShapeDtypeStruct((n,w_out.shape[1]),bf16),jax.ShapeDtypeStruct((n,128),bf16),jax.ShapeDtypeStruct((n,128),bf16)),
        in_specs=[sm]+[vm]*6+[an]*6,
        out_specs=(vm,vm,vm),
        scratch_shapes=[pltpu.VMEM(w_query.shape,bf16),pltpu.VMEM(w_key.shape,bf16),pltpu.VMEM(w_value.shape,bf16),pltpu.VMEM(w_out.shape,bf16),
            pltpu.VMEM(key_cache.shape,bf16),pltpu.VMEM(value_cache.shape,bf16),
            pltpu.VMEM((n*8,128),f32),pltpu.VMEM((n,128),f32),pltpu.VMEM((n,128),f32),pltpu.VMEM((n*8,128),f32),
            pltpu.SemaphoreType.DMA((4,)),pltpu.SemaphoreType.DMA((n,)),pltpu.SemaphoreType.DMA((n,))],
        compiler_params=pltpu.CompilerParams(vmem_limit_bytes=62*1024*1024),
        name="attention",
    )(past_lengths,hidden_in,attn_gain.reshape(1,-1),cos,sin,lambdas.reshape(-1,1),head_gain.reshape(1,-1),w_query,w_key,w_value,key_cache,value_cache,w_out)


EPS_SHIFTS = ((0, 0, 1), (0, 0, 3), (1, 0, 0), (3, 0, 0), (0, 1, 0), (1, 0, 1), (3, 3, 3))
PAD = 48
SLOTS = 8
LIVE = 4


def class_of(chip):
    z, y, x = (chip // 16, (chip // 4) % 4, chip % 4)
    return ((x + z + 2 * y) % 4) * 2 + z % 2


def shifted(x, shift):
    pairs = []
    for chip in range(64):
        z, y, w = (chip // 16, (chip // 4) % 4, chip % 4)
        to = ((z - shift[0]) % 4) * 16 + ((y - shift[1]) % 4) * 4 + (w - shift[2]) % 4
        pairs.append((chip, to))
    return lax.ppermute(x, "ep", pairs)


def swapped(x):
    return lax.ppermute(x, "tp", [(0, 1), (1, 0)])


def turned(a, b):
    return lax.dot_general(a, b, (((1,), (1,)), ((), ())), preferred_element_type=f32)


def block_body(gate, up, down, out):
    cols = gate.shape[1]
    row = lax.broadcasted_iota(jnp.int32, (PAD, cols), 0)
    col = lax.broadcasted_iota(jnp.int32, (PAD, cols), 1)
    eye = (row == col).astype(f32).astype(bf16)
    wide = gate.shape[0]
    out[0:PAD, 0:wide] = turned(eye, gate[...]).astype(bf16)
    out[PAD : 2 * PAD, 0:wide] = turned(eye, up[...]).astype(bf16)
    row = lax.broadcasted_iota(jnp.int32, (2 * PAD, 2 * cols), 0)
    col = lax.broadcasted_iota(jnp.int32, (2 * PAD, 2 * cols), 1)
    low = jnp.logical_and(row < cols, col == row)
    high = jnp.logical_and(row >= PAD, jnp.logical_and(col >= cols, col - cols == row - PAD))
    pick = jnp.logical_or(low, high).astype(f32).astype(bf16)
    out[:, wide:] = jnp.dot(pick, down[...], preferred_element_type=f32).astype(bf16)


def spread_body(rank, first, second, hid, gain, vector, ids, out, res, gate):
    n, width = hid.shape
    half = width // 2
    attn = (first[...].astype(f32) + second[...].astype(f32)).astype(bf16).astype(f32)
    residual = hid[...].astype(f32) + attn
    moe = residual * lax.rsqrt(jnp.mean(residual * residual, axis=-1, keepdims=True) + norm_eps)
    moe = (moe * gain[...]).astype(bf16).astype(f32)
    logit = jnp.sum(moe * vector[...].astype(f32), axis=-1, keepdims=True)
    gate[...] = jnp.broadcast_to((1.0 / (1.0 + jnp.exp(-logit))).astype(bf16).astype(f32), gate.shape)
    lower = rank[0] == 0
    res[...] = jnp.where(lower, residual[:, :half], residual[:, half:])
    mine = jnp.where(lower, moe[:, :half], moe[:, half:]).astype(bf16)
    total = out.shape[0]
    corner = (
        lax.broadcasted_iota(jnp.int32, (8, 2), 0) == lax.broadcasted_iota(jnp.int32, (8, 2), 1)
    ).astype(f32)
    named = turned(corner.astype(bf16), ids[...].astype(f32).astype(bf16))
    row = lax.broadcasted_iota(jnp.int32, (total, n), 0)
    token = lax.broadcasted_iota(jnp.int32, (total, n), 1)
    chip = row // SLOTS
    slot = row % SLOTS
    expert = (chip // 2).astype(f32)
    hit = jnp.logical_or(named[0:1, :] == expert, named[1:2, :] == expert).astype(f32)
    before = (
        lax.broadcasted_iota(jnp.int32, (n, n), 0) < lax.broadcasted_iota(jnp.int32, (n, n), 1)
    ).astype(f32)
    earlier = jnp.dot(hit.astype(bf16), before.astype(bf16), preferred_element_type=f32)
    routed = jnp.where(earlier == slot.astype(f32), hit, 0.0)
    always = (token == LIVE * class_of(chip) + slot - LIVE).astype(f32)
    place = jnp.where(slot < LIVE, routed, always).astype(bf16)
    out[...] = jnp.dot(place, mine, preferred_element_type=f32).astype(bf16)


def hidden_body(rank, own, other, gate, up, *rest):
    blocks, (act, routed, dense) = (rest[:-3], rest[-3:])
    width = own.shape[1]
    lower = rank[0] == 0
    head = lax.broadcasted_iota(jnp.int32, (2, 8, width), 1) < LIVE

    def part(k, _):
        at = pl.multiple_of(k * 32, 32)
        to = pl.multiple_of(k * 16, 16)
        a = own[pl.ds(at, 32), :].astype(f32)
        b = other[pl.ds(at, 32), :].astype(f32)
        for x, lanes in ((jnp.where(lower, a, b), 0), (jnp.where(lower, b, a), width)):
            x = x.reshape(2, 2, 8, width)
            even, odd = (x[:, 0], x[:, 1])
            kept = jnp.where(head, even, pltpu.roll(odd, LIVE, 1)).reshape(16, width)
            rest_ = jnp.where(head, pltpu.roll(even, LIVE, 1), odd).reshape(16, width)
            routed[pl.ds(to, 16), lanes : lanes + width] = kept.astype(bf16)
            dense[pl.ds(to, 16), lanes : lanes + width] = rest_.astype(bf16)
        return 0

    lax.fori_loop(0, own.shape[0] // 32, part, 0)
    rows = routed.shape[0]
    cols = gate.shape[1]

    def gated(g, u):
        return (g / (1.0 + jnp.exp(-g)) * u).astype(bf16)

    x = routed[...]
    act[0:rows, 0:cols] = gated(
        jnp.dot(x, gate[...], preferred_element_type=f32),
        jnp.dot(x, up[...], preferred_element_type=f32),
    )
    act[0:rows, cols:] = jnp.zeros((rows, act.shape[1] - cols), bf16)
    x = dense[...]
    act[rows:, :] = gated(
        turned(x, jnp.concatenate([b[0:PAD, 0 : 2 * width] for b in blocks], axis=0)),
        turned(x, jnp.concatenate([b[PAD : 2 * PAD, 0 : 2 * width] for b in blocks], axis=0)),
    )


def down_body(rank, own, other, down, *rest):
    blocks, (out, routed, dense) = (rest[:-3], rest[-3:])
    rows = routed.shape[0]
    cols = down.shape[0] // 2
    width = out.shape[1]
    here = rank[0]
    sums = []
    for ref, core in ((own, here), (other, 1 - here)):
        at = pl.multiple_of(core * cols, 16)
        low = pl.multiple_of(core * PAD, 16)
        m = jnp.dot(ref[0:rows, 0:cols], down[pl.ds(at, cols), :], preferred_element_type=f32)
        wd = jnp.concatenate([b[pl.ds(low, PAD), 2 * width :] for b in blocks], axis=0)
        sums.append((m, jnp.dot(ref[rows:, :], wd, preferred_element_type=f32)))
    routed[...] = sums[0][0] + sums[1][0]
    dense[...] = sums[0][1] + sums[1][1]
    head = lax.broadcasted_iota(jnp.int32, (2, 8, width), 1) < LIVE

    def part(k, _):
        at = pl.multiple_of(k * 16, 16)
        to = pl.multiple_of(k * 32, 32)
        m = routed[pl.ds(at, 16), :].reshape(2, 8, width)
        d = dense[pl.ds(at, 16), :].reshape(2, 8, width)
        even = jnp.where(head, m, pltpu.roll(d, LIVE, 1))
        odd = jnp.where(head, pltpu.roll(m, LIVE, 1), d)
        both = jnp.concatenate([even[0], odd[0], even[1], odd[1]], axis=0)
        out[pl.ds(to, 32), :] = both.astype(bf16)
        return 0

    lax.fori_loop(0, rows // 16, part, 0)


def combine_body(back, res, gate, ids, weights, out):
    n = res.shape[0]
    total = back.shape[0]
    lane = lax.broadcasted_iota(jnp.int32, (n, total), 1)
    token = lax.broadcasted_iota(jnp.int32, (n, total), 0)
    chip = lane // SLOTS
    slot = lane % SLOTS
    expert = chip // 2
    first = (ids[:, 0:1] == expert).astype(f32)
    second = (ids[:, 1:2] == expert).astype(f32)
    after = (
        lax.broadcasted_iota(jnp.int32, (n, n), 1) < lax.broadcasted_iota(jnp.int32, (n, n), 0)
    ).astype(f32)
    earlier = jnp.dot(
        after.astype(bf16), (first + second).astype(bf16), preferred_element_type=f32
    )
    routed = jnp.where(
        earlier == slot.astype(f32), first * weights[:, 0:1] + second * weights[:, 1:2], 0.0
    )
    always = jnp.where(token == LIVE * class_of(chip) + slot - LIVE, gate[:, 0:1], 0.0)
    w = jnp.where(slot < LIVE, routed, always)
    high = w.astype(bf16)
    left = w - high.astype(f32)
    mid = left.astype(bf16)
    low = (left - mid.astype(f32)).astype(bf16)
    parts = jnp.dot(
        jnp.concatenate([high, mid, low], axis=0), back[...], preferred_element_type=f32
    )
    added = parts[0:n] + parts[n : 2 * n] + parts[2 * n :]
    out[...] = (res[...] + added).astype(bf16)


VM = pl.BlockSpec(memory_space=pltpu.VMEM)
SM = pl.BlockSpec(memory_space=pltpu.SMEM)


def local_kernel(body, outs, ins, scalars=0, scratch=(), name=None):
    return pl.pallas_call(
        body,
        out_shape=tuple(jax.ShapeDtypeStruct(s, d) for s, d in outs),
        in_specs=[SM] * scalars + [VM] * (len(ins) - scalars),
        out_specs=tuple(VM for _ in outs),
        scratch_shapes=[pltpu.VMEM(s, d) for s, d in scratch],
        compiler_params=pltpu.CompilerParams(vmem_limit_bytes=40 * 1024 * 1024),
        name=name,
    )(*ins)


def per_device(
    hidden_in,
    past_lengths,
    key_cache,
    value_cache,
    attn_gain,
    w_query,
    w_key,
    w_value,
    lambdas,
    head_gain,
    w_out,
    ffn_gain,
    route_ids,
    route_weights,
    expert_gate,
    expert_up,
    expert_down,
    gate_vector,
    dense_gate,
    dense_up,
    dense_down,
):
    batch_rows, model_width = hidden_in.shape
    half_width = model_width // 2
    ep_count = lax.axis_size("ep")
    rank = lax.axis_index("tp").astype(jnp.int32).reshape(1)
    (block,) = local_kernel(
        block_body,
        [((2 * PAD, model_width + half_width), bf16)],
        (dense_gate, dense_up, dense_down),
        name="block",
    )
    blocks = [block] + [shifted(block, shift) for shift in EPS_SHIFTS]
    own_part, key_new, value_new = attention(
        past_lengths, hidden_in, attn_gain, w_query, w_key, w_value, key_cache, value_cache,
        lambdas, head_gain, w_out,
    )
    total = ep_count * SLOTS
    outgoing, own_residual, mix_gate = local_kernel(
        spread_body,
        [((total, half_width), bf16), ((batch_rows, half_width), f32), ((batch_rows, 128), f32)],
        (
            rank, own_part, swapped(own_part), hidden_in, ffn_gain.reshape(1, -1),
            gate_vector.reshape(1, -1), route_ids,
        ),
        scalars=1,
        name="spread",
    )
    arrived = lax.all_to_all(
        outgoing.reshape(ep_count, SLOTS, half_width), "ep", 0, 0, tiled=True
    ).reshape(total, half_width)
    live = ep_count * LIVE
    hidden = len(blocks) * PAD
    (act,) = local_kernel(
        hidden_body,
        [((2 * live, hidden), bf16)],
        (rank, arrived, swapped(arrived), expert_gate[0], expert_up[0], *blocks),
        scalars=1,
        scratch=[((live, model_width), bf16)] * 2,
        name="hidden",
    )
    (partial_value,) = local_kernel(
        down_body,
        [((total, half_width), bf16)],
        (rank, act, swapped(act), expert_down[0], *blocks),
        scalars=1,
        scratch=[((live, half_width), f32)] * 2,
        name="down",
    )
    back = lax.all_to_all(
        partial_value.reshape(ep_count, SLOTS, half_width), "ep", 0, 0, tiled=True
    ).reshape(total, half_width)
    (mixed_out,) = local_kernel(
        combine_body,
        [((batch_rows, half_width), bf16)],
        (back, own_residual, mix_gate, route_ids, route_weights),
        name="combine",
    )
    return (mixed_out, key_new, value_new)


def solution(mesh):
    return jax.shard_map(
        per_device,
        mesh=mesh,
        in_specs=(
            P("ep", None),
            P("ep"),
            P("ep", None, "tp"),
            P("ep", None, "tp"),
            P(),
            P(None, "tp"),
            P(None, "tp"),
            P(None, "tp"),
            P("tp"),
            P(),
            P("tp", None),
            P(),
            P("ep", None),
            P("ep", None),
            P("ep", None, "tp"),
            P("ep", None, "tp"),
            P("ep", None, "tp"),
            P(),
            P(None, ("ep", "tp")),
            P(None, ("ep", "tp")),
            P("ep", "tp"),
        ),
        out_specs=(P("ep", "tp"), P("ep", "tp"), P("ep", "tp")),
        check_vma=False,
    )
```

time: 211 us -> 135 us (0.64)
  waiting for transfers between devices: 114 us -> 56.8 us
  matrix products: 16.2 us -> 0 us
  Pallas kernels: 18.8 us -> 34.5 us
  between operations: 14.4 us -> 0.82 us
  other arithmetic: 9.33 us -> 1.52 us
  local copies, waits for them, and re-layouts: 8.2 us -> 11.4 us
    all_to_all x4 -> x2, waiting for transfers between devices: 79.6 us -> 31.7 us  [the longest x1 19.4 us: per_device(): lax.all_to_all(partial_value.reshape(ep_count, SLOTS, half_width), 'ep',...]
    all_gather x1 -> x0, waiting for transfers between devices: 32.6 us -> none  [in_one_piece(): filled, at, outs = (lax.all_gather(both, axis, axis=dim, tiled=True), 0, [])]
    ppermute x0 -> x7, waiting for transfers between devices: none -> 22 us  [shifted(): return lax.ppermute(x, 'ep', pairs)]
    dot_general x9 -> x0, matrix products: 16.2 us -> none  [the longest x1 4.35 us: per_device(): jnp.dot(dense_act, dense_down, preferred_element_type=jnp.float32)]
    pallas_call x0 -> x5, Pallas kernels: none -> 14.4 us  [local_kernel(): pl.pallas_call(body, out_shape=tuple((jax.ShapeDtypeStruct(s, d) for s, d...]
    ppermute x0 -> x7, starting transfers between devices: none -> 12.7 us  [shifted(): return lax.ppermute(x, 'ep', pairs)]
    all_to_all x4 -> x2, starting transfers between devices: 28.6 us -> 16.8 us  [the longest x1 12 us: per_device(): lax.all_to_all(outgoing.reshape(ep_count, SLOTS, half_width), 'ep', 0, 0,...]
    unnamed x30 -> x46, local copies, waits for them, and re-layouts: 0.86 us -> 10.1 us
  transfers between devices with their start and end apart: 9 -> 12, of which waited for: 6 -> 8; matrix products, arithmetic and copies ran while one was open for 10% -> 3% of each run, Pallas kernels for 0% -> 1%
where the time goes in v2:
time: 135 us
  waiting for transfers between devices  56.8 us (42%)
  Pallas kernels  34.5 us (26%)
  starting transfers between devices  29.6 us (22%)
  local copies, waits for them, and re-layouts  11.4 us (8%)
  other arithmetic  1.52 us (1%)
    ppermute x7, waiting for transfers between devices, shifted(): return lax.ppermute(x, 'ep', pairs)  22 us
    pallas_call x1, Pallas kernels, attention(): pl.pallas_call(attention_body, out_shape=(jax.ShapeDtypeStruct((n, w_out....  20.1 us
    all_to_all x1, waiting for transfers between devices, per_device(): lax.all_to_all(partial_value.reshape(ep_count, SLOTS, half_width), 'ep',...  19.4 us
    pallas_call x5, Pallas kernels, local_kernel(): pl.pallas_call(body, out_shape=tuple((jax.ShapeDtypeStruct(s, d) for s, d...  14.4 us
    ppermute x7, starting transfers between devices, shifted(): return lax.ppermute(x, 'ep', pairs)  12.7 us
    all_to_all x1, waiting for transfers between devices, per_device(): lax.all_to_all(outgoing.reshape(ep_count, SLOTS, half_width), 'ep', 0, 0,...  12.4 us
    all_to_all x1, starting transfers between devices, per_device(): lax.all_to_all(outgoing.reshape(ep_count, SLOTS, half_width), 'ep', 0, 0,...  12 us
    unnamed x46, local copies, waits for them, and re-layouts  10.1 us
  transfers between devices with their start and end apart: 12, of which 8 were waited for; matrix products, arithmetic and copies ran while one was open for 3% of the time, Pallas kernels for 1%

profile of v2, /device:TPU:0, one launch (start us, length us, event | category | flops | bytes accessed | tf_op | source)
XLA Modules:
  0.0 134.7 jit_solution(13920517531416491561)
XLA Ops:
  0.6 0.7 convert_element_type.3
  1.3 1.3 copy.24.lam
  2.6 0.1 fusion
  2.8 0.7 pad_maximum_fusion
  3.5 0.0 copy-start.15
  3.5 20.1 %attention.1 = (bf16[32,2048]{1,0:T(8,128)(2,1)}, bf16[32,128]{1,0:T(8,128)(2,1)}, bf16[32,128]{1,0:T(8,128)(2,1)}) custom-call(s32[32]{0:T(128)} %lens.1, bf16[32,2048]{1,0:T(8,128)(2,1)} %hid.3, f32[1,2048]{1,0:T(1,128)} %bitcast.17, f32[32,128]{1,0:T(8,128)} %get-tuple-element.18.cos, f32[32,128]{1,0:T(8,128)} %get-tuple-element.19.sin, ...), custom_call_target="tpu_custom_call" | custom-call | tf_op jit(solution)/shard_map/attention/pallas_call | solution.py:102
  23.6 0.1 collective-permute-start
  23.7 0.1 copy.25.ids
  23.8 1.4 %collective-permute-done.second = bf16[32,2048]{1,0:T(8,128)(2,1)S(1)} collective-permute-done((bf16[32,2048]{1,0:T(8,128)(2,1)}, bf16[32,2048]{1,0:T(8,128)(2,1)S(1)}, u32[]{:S(2)}, u32[]{:S(2)}) %collective-permute-start) | collective-permute-done | bytes 131104 | tf_op jit(solution)/shard_map/ppermute | solution.py:136
  25.3 0.9 copy-done.12
  26.2 1.9 %spread.1 = (bf16[512,1024]{1,0:T(8,128)(2,1)}, f32[32,1024]{1,0:T(8,128)S(1)}, f32[32,128]{1,0:T(8,128)S(1)}) custom-call(s32[1]{0:T(128)} %bitcast.rank, bf16[32,2048]{1,0:T(8,128)(2,1)S(1)} %copy-done.12, bf16[32,2048]{1,0:T(8,128)(2,1)S(1)} %collective-permute-done.second, bf16[32,2048]{1,0:T(8,128)(2,1)S(1)} %copy-done.10, f32[1,2048]{1,0:T(1,128)S(1)} %bitcast.16, ...), custom_call_target="tpu_custom_call" | custom-call | tf_op jit(solution)/shard_map/spread/pallas_call | solution.py:300
  28.1 12.0 %all-to-all-start = ((bf16[64,8,1024]{2,1,0:T(8,128)(2,1)}), bf16[64,8,1024]{2,1,0:T(8,128)(2,1)}, u32[]{:S(2)}, u32[]{:S(2)}) async-start(bf16[64,8,1024]{2,1,0:T(8,128)(2,1)} %bitcast.5), calls=%async_computation | async-start | bytes 2097152 | tf_op jit(solution)/shard_map/all_to_all | solution.py:360
  40.1 0.0 copy-start.14
  40.1 0.3 copy.28.gate
  40.4 0.3 copy.29.up
  40.7 1.4 %block.1.rest_0_ = bf16[96,3072]{1,0:T(8,128)(2,1)} custom-call(bf16[2048,44]{1,0:T(8,128)(2,1)S(1)} %copy.28.gate, bf16[2048,44]{1,0:T(8,128)(2,1)S(1)} %copy.29.up, bf16[88,1024]{1,0:T(8,128)(2,1)S(1)} %copy-done.11), custom_call_target="tpu_custom_call" | custom-call | tf_op jit(solution)/shard_map/block/pallas_call | solution.py:300
  42.1 2.7 %collective-permute-start.2 = (bf16[96,3072]{1,0:T(8,128)(2,1)}, bf16[96,3072]{1,0:T(8,128)(2,1)S(1)}, u32[]{:S(2)}, u32[]{:S(2)}) collective-permute-start(bf16[96,3072]{1,0:T(8,128)(2,1)} %block.1.rest_0_), channel_id=1, source_target_pairs={{0,6},{2,0},{4,2},{6,4},{8,14},{10,8},{12,10},{14,12},{16,22},{18,... | collective-permute-start | bytes 1769480 | tf_op jit(solution)/shard_map/ppermute | solution.py:132
  44.8 0.0 collective-permute-start.3
  44.8 2.9 %collective-permute-start.4 = (bf16[96,3072]{1,0:T(8,128)(2,1)}, bf16[96,3072]{1,0:T(8,128)(2,1)S(1)}, u32[]{:S(2)}, u32[]{:S(2)}) collective-permute-start(bf16[96,3072]{1,0:T(8,128)(2,1)} %block.1.rest_0_), channel_id=1, source_target_pairs={{0,96},{2,98},{4,100},{6,102},{8,104},{10,106},{12,108},{14,110},{... | collective-permute-start | bytes 1769480 | tf_op jit(solution)/shard_map/ppermute | solution.py:132
  47.7 12.4 %all-to-all-done = bf16[64,8,1024]{2,1,0:T(8,128)(2,1)} async-done(((bf16[64,8,1024]{2,1,0:T(8,128)(2,1)}), bf16[64,8,1024]{2,1,0:T(8,128)(2,1)}, u32[]{:S(2)}, u32[]{:S(2)}) %all-to-all-start) | async-done | bytes 1048608 | tf_op jit(solution)/shard_map/all_to_all | solution.py:360
  60.1 0.0 collective-permute-start.1
  60.1 0.2 collective-permute-start.5
  60.3 5.2 %collective-permute-done.2.rest_1_ = bf16[96,3072]{1,0:T(8,128)(2,1)S(1)} collective-permute-done((bf16[96,3072]{1,0:T(8,128)(2,1)}, bf16[96,3072]{1,0:T(8,128)(2,1)S(1)}, u32[]{:S(2)}, u32[]{:S(2)}) %collective-permute-start.2) | collective-permute-done | bytes 589856 | tf_op jit(solution)/shard_map/ppermute | solution.py:132
  65.6 0.8 copy-done
  66.4 2.7 %collective-permute-start.6 = (bf16[96,3072]{1,0:T(8,128)(2,1)}, bf16[96,3072]{1,0:T(8,128)(2,1)}, u32[]{:S(2)}, u32[]{:S(2)}) collective-permute-start(bf16[96,3072]{1,0:T(8,128)(2,1)} %block.1.rest_0_), channel_id=1, source_target_pairs={{0,24},{2,26},{4,28},{6,30},{8,0},{10,2},{12,4},{14,6},{16,8},{18,... | collective-permute-start | bytes 1769480 | tf_op jit(solution)/shard_map/ppermute | solution.py:132
  69.1 0.0 collective-permute-done.3.rest_2_
  69.1 0.8 copy-done.3
  69.9 4.2 %collective-permute-start.7 = (bf16[96,3072]{1,0:T(8,128)(2,1)}, bf16[96,3072]{1,0:T(8,128)(2,1)}, u32[]{:S(2)}, u32[]{:S(2)}) collective-permute-start(bf16[96,3072]{1,0:T(8,128)(2,1)} %block.1.rest_0_), channel_id=1, source_target_pairs={{0,102},{2,96},{4,98},{6,100},{8,110},{10,104},{12,106},{14,108},{... | collective-permute-start | bytes 1769480 | tf_op jit(solution)/shard_map/ppermute | solution.py:132
  74.1 0.8 copy-done.6
  74.9 0.0 collective-permute-start.8
  74.9 0.8 copy.26
  75.8 1.9 %copy.27 = bf16[1,2048,352]{2,1,0:T(8,128)(2,1)S(1)} copy(bf16[1,2048,352]{1,2,0:T(8,128)(2,1)} %param.36) | data formatting | bytes 2883584 | tf_op args[15]
  77.6 0.0 collective-permute-done.5.rest_4_
  77.6 3.6 %collective-permute-done.6.rest_5_ = bf16[96,3072]{1,0:T(8,128)(2,1)} collective-permute-done((bf16[96,3072]{1,0:T(8,128)(2,1)}, bf16[96,3072]{1,0:T(8,128)(2,1)}, u32[]{:S(2)}, u32[]{:S(2)}) %collective-permute-start.6) | collective-permute-done | bytes 589856 | tf_op jit(solution)/shard_map/ppermute | solution.py:132
  81.3 4.6 %collective-permute-done.7.rest_6_ = bf16[96,3072]{1,0:T(8,128)(2,1)} collective-permute-done((bf16[96,3072]{1,0:T(8,128)(2,1)}, bf16[96,3072]{1,0:T(8,128)(2,1)}, u32[]{:S(2)}, u32[]{:S(2)}) %collective-permute-start.7) | collective-permute-done | bytes 589856 | tf_op jit(solution)/shard_map/ppermute | solution.py:132
  85.9 8.5 %collective-permute-done.8.rest_7_ = bf16[96,3072]{1,0:T(8,128)(2,1)} collective-permute-done((bf16[96,3072]{1,0:T(8,128)(2,1)}, bf16[96,3072]{1,0:T(8,128)(2,1)}, u32[]{:S(2)}, u32[]{:S(2)}) %collective-permute-start.8) | collective-permute-done | bytes 589856 | tf_op jit(solution)/shard_map/ppermute | solution.py:132
  94.3 0.0 collective-permute-done.1.other
  94.3 1.1 copy-done.1
  95.4 1.1 copy-done.4
  96.5 1.1 copy-done.7
  97.6 5.7 %hidden.1.own = bf16[512,384]{1,0:T(8,128)(2,1)S(1)} custom-call(s32[1]{0:T(128)} %bitcast.rank, bf16[512,1024]{1,0:T(8,128)(2,1)} %bitcast.6.own, bf16[512,1024]{1,0:T(8,128)(2,1)} %collective-permute-done.1.other, bf16[2048,352]{1,0:T(8,128)(2,1)S(1)} %bitcast.12, bf16[2048,352]{1,0:T(8,128)(2,1)S(1)} %bitcast.13, bf16[96,3072]{1,0:T(8,128)(2,1)} %block.1.rest_0_, ...), custom_call_target="tpu_custom_call" | custom-call | tf_op jit(solution)/shard_map/hidden/pallas_call | solution.py:300
  103.3 0.1 collective-permute-start.9
  103.4 1.7 %collective-permute-done.9.other = bf16[512,384]{1,0:T(8,128)(2,1)S(1)} collective-permute-done((bf16[512,384]{1,0:T(8,128)(2,1)S(1)}, bf16[512,384]{1,0:T(8,128)(2,1)S(1)}, u32[]{:S(2)}, u32[]{:S(2)}) %collective-permute-start.9) | collective-permute-done | bytes 393248 | tf_op jit(solution)/shard_map/ppermute | solution.py:136
  105.1 4.2 %down.3 = bf16[512,1024]{1,0:T(8,128)(2,1)} custom-call(s32[1]{0:T(128)} %bitcast.rank, bf16[512,384]{1,0:T(8,128)(2,1)S(1)} %hidden.1.own, bf16[512,384]{1,0:T(8,128)(2,1)S(1)} %collective-permute-done.9.other, bf16[704,1024]{1,0:T(8,128)(2,1)S(1)} %bitcast.15, bf16[96,3072]{1,0:T(8,128)(2,1)} %block.1.rest_0_, bf16[96,3072]{1,0:T(8,128)(2,1)S(1)} %copy-done.2, ...), custom_call_target="tpu_custom_call" | custom-call | tf_op jit(solution)/shard_map/down/pallas_call | solution.py:300
  109.3 4.8 %all-to-all-start.1 = ((bf16[64,8,1024]{2,1,0:T(8,128)(2,1)}), bf16[64,8,1024]{2,1,0:T(8,128)(2,1)S(1)}, u32[]{:S(2)}, u32[]{:S(2)}) async-start(bf16[64,8,1024]{2,1,0:T(8,128)(2,1)} %bitcast.10), calls=%async_computation.1 | async-start | bytes 2097152 | tf_op jit(solution)/shard_map/all_to_all | solution.py:381
  114.1 0.1 copy.31.weights
  114.2 19.4 %all-to-all-done.1 = bf16[64,8,1024]{2,1,0:T(8,128)(2,1)S(1)} async-done(((bf16[64,8,1024]{2,1,0:T(8,128)(2,1)}), bf16[64,8,1024]{2,1,0:T(8,128)(2,1)S(1)}, u32[]{:S(2)}, u32[]{:S(2)}) %all-to-all-start.1) | async-done | bytes 1048608 | tf_op jit(solution)/shard_map/all_to_all | solution.py:381
  133.6 1.1 combine.1
  (34 shorter events, 0.1 us)
Async XLA Ops:
  3.5 20.3 %copy-start.18 = (s32[32,2]{0,1:T(2,128)S(1)}, s32[32,2]{0,1:T(2,128)}, u32[]{:S(2)}) copy-start(s32[32,2]{0,1:T(2,128)} %param.33) | copy-start | bytes 772
  3.5 20.4 %copy-start.17 = (bf16[2048]{0:T(1024)(128)(2,1)S(1)}, bf16[2048]{0:T(1024)(128)(2,1)}, u32[]{:S(2)}) copy-start(bf16[2048]{0:T(1024)(128)(2,1)} %param.38) | copy-start | bytes 12292
  3.5 21.8 %copy-start.10 = (bf16[32,2048]{1,0:T(8,128)(2,1)S(1)}, bf16[32,2048]{1,0:T(8,128)(2,1)}, u32[]{:S(2)}) copy-start(bf16[32,2048]{1,0:T(8,128)(2,1)} %hid.3) | copy-start | bytes 393220
  3.5 21.8 %copy-start.13 = (f32[2048]{0:T(1024)S(1)}, f32[2048]{0:T(1024)}, u32[]{:S(2)}) copy-start(f32[2048]{0:T(1024)} %param.32) | copy-start | bytes 24580
  3.5 36.6 %copy-start.15 = (bf16[2048,44]{0,1:T(8,128)(2,1)S(1)}, bf16[2048,44]{0,1:T(8,128)(2,1)}, u32[]{:S(2)}) copy-start(bf16[2048,44]{0,1:T(8,128)(2,1)} %param.39) | copy-start | bytes 540676
  23.6 1.6 %collective-permute-start = (bf16[32,2048]{1,0:T(8,128)(2,1)}, bf16[32,2048]{1,0:T(8,128)(2,1)S(1)}, u32[]{:S(2)}, u32[]{:S(2)}) collective-permute-start(bf16[32,2048]{1,0:T(8,128)(2,1)} %get-tuple-element.9.first), channel_id=1, source_target_pairs={{0,1},{1,0},{2,3},{3,2},{4,5},{5,4},{6,7},{7,6},{8,9},{9,8},{10,11... | collective-permute-start | bytes 393224 | tf_op jit(solution)/shard_map/ppermute | solution.py:136
  25.3 0.9 copy-start.12
  28.1 12.3 %copy-start.16 = (bf16[2048,44]{0,1:T(8,128)(2,1)S(1)}, bf16[2048,44]{0,1:T(8,128)(2,1)}, u32[]{:S(2)}) copy-start(bf16[2048,44]{0,1:T(8,128)(2,1)} %param.40) | copy-start | bytes 540676
  28.1 12.6 %copy-start.11 = (bf16[88,1024]{1,0:T(8,128)(2,1)S(1)}, bf16[88,1024]{1,0:T(8,128)(2,1)}, u32[]{:S(2)}) copy-start(bf16[88,1024]{1,0:T(8,128)(2,1)} %down.2) | copy-start | bytes 540676
  28.1 31.9 %all-to-all-start = ((bf16[64,8,1024]{2,1,0:T(8,128)(2,1)}), bf16[64,8,1024]{2,1,0:T(8,128)(2,1)}, u32[]{:S(2)}, u32[]{:S(2)}) async-start(bf16[64,8,1024]{2,1,0:T(8,128)(2,1)} %bitcast.5), calls=%async_computation | async-start | bytes 2097152 | tf_op jit(solution)/shard_map/all_to_all | solution.py:360
  40.1 34.8 %copy-start.14 = (bf16[1,2048,352]{1,2,0:T(8,128)(2,1)S(1)}, bf16[1,2048,352]{1,2,0:T(8,128)(2,1)}, u32[]{:S(2)}) copy-start(bf16[1,2048,352]{1,2,0:T(8,128)(2,1)} %param.35) | copy-start | bytes 4325380
  42.1 23.5 %collective-permute-start.2 = (bf16[96,3072]{1,0:T(8,128)(2,1)}, bf16[96,3072]{1,0:T(8,128)(2,1)S(1)}, u32[]{:S(2)}, u32[]{:S(2)}) collective-permute-start(bf16[96,3072]{1,0:T(8,128)(2,1)} %block.1.rest_0_), channel_id=1, source_target_pairs={{0,6},{2,0},{4,2},{6,4},{8,14},{10,8},{12,10},{14,12},{16,22},{18,... | collective-permute-start | bytes 1769480 | tf_op jit(solution)/shard_map/ppermute | solution.py:132
  44.8 24.3 %collective-permute-start.3 = (bf16[96,3072]{1,0:T(8,128)(2,1)}, bf16[96,3072]{1,0:T(8,128)(2,1)S(1)}, u32[]{:S(2)}, u32[]{:S(2)}) collective-permute-start(bf16[96,3072]{1,0:T(8,128)(2,1)} %block.1.rest_0_), channel_id=1, source_target_pairs={{0,2},{2,4},{4,6},{6,0},{8,10},{10,12},{12,14},{14,8},{16,18},{18,... | collective-permute-start | bytes 1769480 | tf_op jit(solution)/shard_map/ppermute | solution.py:132
  44.8 29.3 %collective-permute-start.4 = (bf16[96,3072]{1,0:T(8,128)(2,1)}, bf16[96,3072]{1,0:T(8,128)(2,1)S(1)}, u32[]{:S(2)}, u32[]{:S(2)}) collective-permute-start(bf16[96,3072]{1,0:T(8,128)(2,1)} %block.1.rest_0_), channel_id=1, source_target_pairs={{0,96},{2,98},{4,100},{6,102},{8,104},{10,106},{12,108},{14,110},{... | collective-permute-start | bytes 1769480 | tf_op jit(solution)/shard_map/ppermute | solution.py:132
  60.1 34.3 %collective-permute-start.1 = (bf16[512,1024]{1,0:T(8,128)(2,1)}, bf16[512,1024]{1,0:T(8,128)(2,1)}, u32[]{:S(2)}, u32[]{:S(2)}) collective-permute-start(bf16[512,1024]{1,0:T(8,128)(2,1)} %bitcast.6.own), channel_id=1, source_target_pairs={{0,1},{1,0},{2,3},{3,2},{4,5},{5,4},{6,7},{7,6},{8,9},{9,8},{10,11... | collective-permute-start | bytes 3145736 | tf_op jit(solution)/shard_map/ppermute | solution.py:136
  60.1 17.6 %collective-permute-start.5 = (bf16[96,3072]{1,0:T(8,128)(2,1)}, bf16[96,3072]{1,0:T(8,128)(2,1)}, u32[]{:S(2)}, u32[]{:S(2)}) collective-permute-start(bf16[96,3072]{1,0:T(8,128)(2,1)} %block.1.rest_0_), channel_id=1, source_target_pairs={{0,32},{2,34},{4,36},{6,38},{8,40},{10,42},{12,44},{14,46},{16,48}... | collective-permute-start | bytes 1769480 | tf_op jit(solution)/shard_map/ppermute | solution.py:132
  65.6 0.8 copy-start
  66.4 14.9 %collective-permute-start.6 = (bf16[96,3072]{1,0:T(8,128)(2,1)}, bf16[96,3072]{1,0:T(8,128)(2,1)}, u32[]{:S(2)}, u32[]{:S(2)}) collective-permute-start(bf16[96,3072]{1,0:T(8,128)(2,1)} %block.1.rest_0_), channel_id=1, source_target_pairs={{0,24},{2,26},{4,28},{6,30},{8,0},{10,2},{12,4},{14,6},{16,8},{18,... | collective-permute-start | bytes 1769480 | tf_op jit(solution)/shard_map/ppermute | solution.py:132
  69.1 0.8 copy-start.3
  69.9 16.0 %collective-permute-start.7 = (bf16[96,3072]{1,0:T(8,128)(2,1)}, bf16[96,3072]{1,0:T(8,128)(2,1)}, u32[]{:S(2)}, u32[]{:S(2)}) collective-permute-start(bf16[96,3072]{1,0:T(8,128)(2,1)} %block.1.rest_0_), channel_id=1, source_target_pairs={{0,102},{2,96},{4,98},{6,100},{8,110},{10,104},{12,106},{14,108},{... | collective-permute-start | bytes 1769480 | tf_op jit(solution)/shard_map/ppermute | solution.py:132
  74.1 0.8 copy-start.6
  74.9 19.4 %collective-permute-start.8 = (bf16[96,3072]{1,0:T(8,128)(2,1)}, bf16[96,3072]{1,0:T(8,128)(2,1)}, u32[]{:S(2)}, u32[]{:S(2)}) collective-permute-start(bf16[96,3072]{1,0:T(8,128)(2,1)} %block.1.rest_0_), channel_id=1, source_target_pairs={{0,42},{2,44},{4,46},{6,40},{8,50},{10,52},{12,54},{14,48},{16,58}... | collective-permute-start | bytes 1769480 | tf_op jit(solution)/shard_map/ppermute | solution.py:132
  94.3 1.1 copy-start.1
  95.4 1.1 copy-start.4
  96.5 1.1 copy-start.7
  97.5 7.5 %copy-start.2 = (bf16[96,3072]{1,0:T(8,128)(2,1)S(1)}, bf16[96,3072]{1,0:T(8,128)(2,1)}, u32[]{:S(2)}) copy-start(bf16[96,3072]{1,0:T(8,128)(2,1)} %copy-done) | copy-start | bytes 1769476
  97.5 7.5 %copy-start.5 = (bf16[96,3072]{1,0:T(8,128)(2,1)S(1)}, bf16[96,3072]{1,0:T(8,128)(2,1)}, u32[]{:S(2)}) copy-start(bf16[96,3072]{1,0:T(8,128)(2,1)} %copy-done.3) | copy-start | bytes 1769476
  97.5 7.5 %copy-start.8 = (bf16[96,3072]{1,0:T(8,128)(2,1)S(1)}, bf16[96,3072]{1,0:T(8,128)(2,1)}, u32[]{:S(2)}) copy-start(bf16[96,3072]{1,0:T(8,128)(2,1)} %copy-done.6) | copy-start | bytes 1769476
  97.5 7.5 %copy-start.9 = (bf16[1,704,1024]{2,1,0:T(8,128)(2,1)S(1)}, bf16[1,704,1024]{2,1,0:T(8,128)(2,1)}, u32[]{:S(2)}) copy-start(bf16[1,704,1024]{2,1,0:T(8,128)(2,1)} %param.37) | copy-start | bytes 4325380
  103.3 1.8 %collective-permute-start.9 = (bf16[512,384]{1,0:T(8,128)(2,1)S(1)}, bf16[512,384]{1,0:T(8,128)(2,1)S(1)}, u32[]{:S(2)}, u32[]{:S(2)}) collective-permute-start(bf16[512,384]{1,0:T(8,128)(2,1)S(1)} %hidden.1.own), channel_id=1, source_target_pairs={{0,1},{1,0},{2,3},{3,2},{4,5},{5,4},{6,7},{7,6},{8,9},{9,8},{10,11... | collective-permute-start | bytes 1179656 | tf_op jit(solution)/shard_map/ppermute | solution.py:136
  109.3 4.8 %copy-start.19 = (f32[32,2]{0,1:T(2,128)S(1)}, f32[32,2]{0,1:T(2,128)}, u32[]{:S(2)}) copy-start(f32[32,2]{0,1:T(2,128)} %param.34) | copy-start | bytes 772
  109.3 24.3 %all-to-all-start.1 = ((bf16[64,8,1024]{2,1,0:T(8,128)(2,1)}), bf16[64,8,1024]{2,1,0:T(8,128)(2,1)S(1)}, u32[]{:S(2)}, u32[]{:S(2)}) async-start(bf16[64,8,1024]{2,1,0:T(8,128)(2,1)} %bitcast.10), calls=%async_computation.1 | async-start | bytes 2097152 | tf_op jit(solution)/shard_map/all_to_all | solution.py:381
